TPU v7x, 32 devices: a whole 2x2x4 slice. The times are simulated.
32 devices in a mesh: sp: 16 (over z, y, x), tp: 2 (over core).
Axes of the slice: x: 2, y: 2, z: 4, core: 2. Of those that a mesh axis runs over, the one named last changes fastest.
Arguments:
- tokens: bfloat16 [16384, 2048], P('sp', 'tp'), may hold values from -6 to 6
- norm_gain: float32 [2048], replicated, may hold values from 0.1 to 1.9
- w_conv_a: bfloat16 [2048, 1024], P('sp', 'tp'), may hold values from -0.125 to 0.125
- w_conv_gate: bfloat16 [2048, 1024], P('sp', 'tp'), may hold values from -0.125 to 0.125
- conv_weight: float32 [31, 1024], P(None, 'tp'), may hold values from -16 to 16
- conv_gain: float32 [1024], P('tp'), may hold values from 0.1 to 1.9
- w_query: bfloat16 [2048, 512], P('sp', 'tp'), may hold values from -0.125 to 0.125
- w_key: bfloat16 [2048, 512], P('sp', 'tp'), may hold values from -0.125 to 0.125
- w_value: bfloat16 [2048, 1024], P('sp', 'tp'), may hold values from -0.125 to 0.125
- w_outgate: bfloat16 [2048, 1024], P('sp', 'tp'), may hold values from -0.125 to 0.125
- w_decay: bfloat16 [2048, 512], P('sp', 'tp'), may hold values from -0.125 to 0.125
- decay_bias: float32 [512], P('tp'), may hold values from 0 to 12
- decay_extra: float32 [16384, 512], P('sp', 'tp'), may hold values from -2 to 0
- head_gain: float32 [128], replicated, may hold values from 0.1 to 1.9
- init_state: float32 [8, 64, 128], P('tp'), may hold values from -768 to 768
- w_out_conv: bfloat16 [1024, 2048], P('tp', 'sp'), may hold values from -0.125 to 0.125
- w_out_gla: bfloat16 [1024, 2048], P('tp', 'sp'), may hold values from -0.125 to 0.125
Outputs:
- mixed: bfloat16 [16384, 2048], P(('sp', 'tp'))
All inputs are finite; a program needn't handle non-finite values.
Results may differ from a plain program's by a relative error of at most 0.022.
Values may be sent and summed in bfloat16 or wider, within the bound.
A program may use at most 128 MiB of HBM per device.

v0:
```python
import functools

import jax
import jax.numpy as jnp
from jax import lax
from jax.experimental import pallas as pl
from jax.experimental.pallas import tpu as pltpu
from jax.sharding import PartitionSpec as P

D_CONV = 1024
HK = 64
HV = 128
BLOCK = 64

epsilon = 1e-06
gate_divisor = 16.0

MESH = pl.DeviceIdType.MESH


def dot(a, b, dims):
    return lax.dot_general(a, b, (dims, ((), ())), preferred_element_type=jnp.float32)


def folded(n_sp, n_tp):
    return n_sp == 16 and n_tp == 2


class Mover:
    def __init__(self):
        self.me = lax.axis_index("sp")
        self.tp = lax.axis_index("tp")
        self.z, self.y, self.x = self.me // 4, (self.me // 2) % 2, self.me % 2
        self.other = {"x": self.me + 1 - 2 * self.x, "y": self.me + 2 - 4 * self.y}
        self.sent = []

    def copy(self, source, target, send, recv, place, core=None):
        core = self.tp if core is None else core
        return pltpu.make_async_remote_copy(
            src_ref=source, dst_ref=target, send_sem=send, recv_sem=recv, device_id=(place, core), device_id_type=MESH
        )

    def piece(self, j):
        z = self.z
        return (z, z + 1 - 2 * (z % 2), 2 - z // 2, 3 - 3 * (z // 2))[j]


class Flow:
    def __init__(self, mover, number, view, first, sems):
        self.m, self.number, self.view, self.first = mover, number, view, first
        self.last = {"x": "y", "y": "x"}[first]
        self.sems = sems

    def own(self, p):
        return self.view(p, self.m.y, self.m.x)

    def pair(self, p):
        every = slice(None)
        return self.view(p, self.m.y, every) if self.first == "x" else self.view(p, every, self.m.x)

    def first_copy(self, p):
        own = self.own(p)
        fs, fr = self.sems["first_send"], self.sems["first_recv"]
        return self.m.copy(own, own, fs.at[self.number, p], fr.at[self.number, p], self.m.other[self.first])

    def last_copy(self, p):
        pair = self.pair(p)
        ls, lr = self.sems["last_send"], self.sems["last_recv"]
        return self.m.copy(pair, pair, ls.at[self.number, p], lr.at[self.number, p], self.m.other[self.last])


class Line:
    def __init__(self, mover, number, view, sems):
        self.m, self.number, self.view, self.sems = mover, number, view, sems

    def up(self, p):
        return self.m.copy(
            self.view(p), self.view(p), self.sems["up_send"].at[self.number, p], self.sems["z_recv"].at[self.number, p],
            self.m.me + 4,
        )

    def down(self, p):
        return self.m.copy(
            self.view(p), self.view(p), self.sems["down_send"].at[self.number, p],
            self.sems["z_recv"].at[self.number, p], self.m.me - 4,
        )

    def start_own(self):
        z = self.m.z

        @pl.when(z < 3)
        def _():
            self.up(z).start()

        @pl.when(z > 0)
        def _():
            self.down(z).start()

    def relay(self, step, then):
        z = self.m.z

        @pl.when(z >= step)
        def _():
            p = z - step
            self.up(p).wait_recv()

            @pl.when(z < 3)
            def _():
                self.up(p).start()

            then(p)

        @pl.when(z + step <= 3)
        def _():
            p = z + step
            self.down(p).wait_recv()

            @pl.when(z > 0)
            def _():
                self.down(p).start()

            then(p)

    def drain(self):
        z = self.m.z
        for p in range(4):
            @pl.when((p <= z) & (z < 3))
            def _():
                self.up(p).wait_send()

            @pl.when((p >= z) & (z > 0))
            def _():
                self.down(p).wait_send()


def at_step(z, step, then):
    if step == 0:
        then(z)
        return

    @pl.when(z >= step)
    def _():
        then(z - step)

    @pl.when(z + step <= 3)
    def _():
        then(z + step)


def layer_kernel(
    tokens, gain, wa, wg, taps, conv_gain, wq, wk, wv, wog, wd, bias, extra_in, head_gain, init, woc, wogl, out,
    w1, w2, w3, wo, both, normed, acc1, acc2, acc3, extra, seq, attn, since, act, psend, pown, precv, outv,
    halo_out, halo_in, stat_own, stat_in, packs, state, prefix, before,
    local, first_send, first_recv, last_send, last_recv, up_send, down_send, z_recv, misc_send, misc_recv, end_send, end_recv,
    part_send, part_recv, out_sem,
):
    m = Mover()
    me, tp, z, y, x = m.me, m.tp, m.z, m.y, m.x
    rows = normed.shape[0]
    half = rows // 2
    width = both.shape[2]
    n_key = acc1.shape[1] // 5
    n_conv = 2 * n_key
    heads = n_key // HK
    sems = dict(
        first_send=first_send, first_recv=first_recv, last_send=last_send, last_recv=last_recv,
        up_send=up_send, down_send=down_send, z_recv=z_recv,
    )

    def lanes(ref, low, size):
        return lambda p, yy, xx: ref.at[p, yy, xx, :, pl.ds(low, size)]

    def depth(low, size):
        return lambda p, yy, xx: wo.at[p, yy, xx, pl.ds(low, size), :]

    mid = w1.shape[-1] // 2
    b1 = Flow(m, 0, lanes(w1, 0, mid), "x", sems)
    b2 = Flow(m, 1, lanes(w1, mid, mid), "y", sems)
    pairs = [
        (Flow(m, 2, lanes(w2, 0, n_conv), "x", sems), Flow(m, 3, lanes(w2, n_conv, n_conv), "y", sems)),
        (Flow(m, 4, lanes(w3, 0, n_key), "x", sems), Flow(m, 5, lanes(w3, n_key, n_key), "y", sems)),
        (Flow(m, 6, depth(0, n_conv), "x", sems), Flow(m, 7, depth(n_conv, n_conv), "y", sems)),
    ]
    whole = Line(m, 0, lambda p: w1.at[p, y, x], sems)
    lines = [tuple(Line(m, f.number - 1, f.pair, sems) for f in pair) for pair in pairs]

    loads = [
        (wq, w1.at[z, y, x, :, pl.ds(0, n_key)]),
        (wk, w1.at[z, y, x, :, pl.ds(n_key, n_key)]),
        (wd, w1.at[z, y, x, :, pl.ds(2 * n_key, n_key)]),
        (wv, w1.at[z, y, x, :, pl.ds(3 * n_key, n_conv)]),
        (wa, w2.at[z, y, x, :, pl.ds(0, n_conv)]),
        (wg, w2.at[z, y, x, :, pl.ds(n_conv, n_conv)]),
        (wog, w3.at[z, y, x]),
        (woc, wo.at[z, y, x, pl.ds(0, n_conv), :]),
        (wogl, wo.at[z, y, x, pl.ds(n_conv, n_conv), :]),
        (tokens, both.at[tp]),
        (extra_in, extra),
    ]
    loads = [pltpu.make_async_copy(a, b, local.at[i]) for i, (a, b) in enumerate(loads)]
    for load in loads:
        load.start()

    barrier = pltpu.get_barrier_semaphore()
    partners = [(m.other["x"], tp), (m.other["y"], tp), (me, 1 - tp)]
    partners += [((me + k) % 16, tp) for k in (4, 8, 12, 1, 15)]
    for place, core in partners:
        pl.semaphore_signal(barrier, inc=1, device_id=(place, core), device_id_type=MESH)
    pl.semaphore_wait(barrier, len(partners))

    for i in range(4):
        loads[i].wait()
    whole.start_own()
    b1.first_copy(z).start()
    b2.first_copy(z).start()
    loads[9].wait()
    swap = m.copy(both.at[tp], both.at[tp], misc_send.at[0], misc_recv.at[0], me, 1 - tp)
    swap.start()
    loads[4].wait()
    loads[5].wait()
    for f in pairs[0]:
        f.first_copy(z).start()
    for i in (6, 7, 8):
        loads[i].wait()
    for pair in pairs[1:]:
        for f in pair:
            f.first_copy(z).start()
    loads[10].wait()

    def head_firsts(step):
        def one(p):
            b1.first_copy(p).wait_recv()
            b1.last_copy(p).start()
            b2.first_copy(p).wait_recv()
            b2.last_copy(p).start()

        at_step(z, step, one)

    def head_line(step):
        def then(p):
            b1.first_copy(p).start()
            b2.first_copy(p).start()

        whole.relay(step, then)

    def enter(k):
        for f, line in zip(pairs[k], lines[k]):
            f.first_copy(z).wait_recv()
            line.start_own()
            f.last_copy(z).start()

    def pass_on(k, step):
        for f, line in zip(pairs[k], lines[k]):
            line.relay(step, lambda p: f.last_copy(p).start())

    def arrived(flows, p):
        for f in flows:
            f.last_copy(p).wait_recv()

    def norm_tiles(low, high):
        def body(i, carry):
            at = pl.ds(pl.multiple_of(i * 128, 128), 128)
            a = both[0, at, :].astype(jnp.float32)
            b = both[1, at, :].astype(jnp.float32)
            square = jnp.sum(a * a + b * b, axis=1, keepdims=True)
            scale = lax.rsqrt(square / (2 * width) + epsilon)
            normed[at, :width] = (a * scale * gain[:, :width]).astype(jnp.bfloat16)
            normed[at, width:] = (b * scale * gain[:, width:]).astype(jnp.bfloat16)
            return carry

        lax.fori_loop(low, high, body, 0)

    def slab(acc, ref, p, first):
        size = ref.shape[1] * ref.shape[2] * ref.shape[3]

        def body(c, carry):
            at = pl.ds(pl.multiple_of(c * 256, 256), 256)
            left = normed[:, pl.ds(pl.multiple_of(p * size, size), size)]
            right = ref[p, :, :, :, at].reshape(size, 256)
            got = dot(left, right, ((1,), (0,)))
            if first:
                acc[:, at] = got
            else:
                acc[:, at] += got
            return carry

        lax.fori_loop(0, acc.shape[1] // 256, body, 0)

    swap.wait_recv()
    norm_tiles(0, 4)
    head_line(1)
    head_firsts(0)
    norm_tiles(4, 8)
    head_line(2)
    enter(0)
    head_firsts(1)
    head_line(3)
    head_firsts(2)
    arrived((b1, b2), m.piece(0))
    slab(acc1, w1, m.piece(0), True)
    head_firsts(3)
    arrived((b1, b2), m.piece(1))
    slab(acc1, w1, m.piece(1), False)
    pass_on(0, 1)
    arrived((b1, b2), m.piece(2))
    slab(acc1, w1, m.piece(2), False)
    pass_on(0, 2)
    enter(1)
    arrived((b1, b2), m.piece(3))
    slab(acc1, w1, m.piece(3), False)

    state[...] = jnp.zeros_like(state)
    prefix[...] = jnp.zeros_like(prefix)
    r_iota = lax.broadcasted_iota(jnp.int32, (BLOCK, BLOCK), 0)
    c_iota = lax.broadcasted_iota(jnp.int32, (BLOCK, BLOCK), 1)
    causal = r_iota >= c_iota
    lower = causal.astype(jnp.float32)

    def block(i, carry):
        at = pl.ds(pl.multiple_of(i * BLOCK, BLOCK), BLOCK)
        pre = acc1[at, 2 * n_key : 3 * n_key] + bias[...]
        logs = jax.nn.log_sigmoid(pre) / gate_divisor + extra[at, :]
        cum = lax.dot_general(
            lower, logs, (((1,), (0,)), ((), ())), precision=lax.Precision.HIGHEST, preferred_element_type=jnp.float32
        )
        total = cum[BLOCK - 1 :, :]
        middle = cum[BLOCK // 2 - 1 : BLOCK // 2, :]
        query = acc1[at, 0:n_key].astype(jnp.bfloat16).astype(jnp.float32) * HK ** (-0.5)
        keys = acc1[at, n_key : 2 * n_key].astype(jnp.bfloat16).astype(jnp.float32)
        decayed = query * jnp.exp(cum)
        since[at, :] = (decayed * jnp.exp(prefix[...])).astype(jnp.bfloat16)
        decayed = decayed.astype(jnp.bfloat16)
        query = (query * jnp.exp(cum - middle)).astype(jnp.bfloat16)
        inverse = (keys * jnp.exp(middle - cum)).astype(jnp.bfloat16)
        to_end = (keys * jnp.exp(total - cum)).astype(jnp.bfloat16)
        entering = state[...].astype(jnp.bfloat16)
        added = []
        for h in range(heads):
            ks, vs = slice(h * HK, (h + 1) * HK), slice(h * HV, (h + 1) * HV)
            values = acc1[at, 3 * n_key + h * HV : 3 * n_key + (h + 1) * HV].astype(jnp.bfloat16)
            scores = jnp.where(causal, dot(query[:, ks], inverse[:, ks], ((1,), (1,))), 0.0)
            attn[at, vs] = dot(scores.astype(jnp.bfloat16), values, ((1,), (0,))) + dot(
                decayed[:, ks], entering[:, ks], ((1,), (1,))
            )
            added.append(dot(values, to_end[:, ks], ((0,), (0,))))
        state[...] = state[...] * jnp.exp(total) + jnp.concatenate(added, axis=1)
        prefix[...] = prefix[...] + total
        return carry

    blocks = rows // BLOCK
    quarter = blocks // 4

    def attend(i, carry):
        block(i, 0)

        @pl.when(i == quarter)
        def _():
            pass_on(0, 3)

        @pl.when(i == 3 * quarter)
        def _():
            pass_on(1, 1)

        return carry

    lax.fori_loop(0, blocks, attend, 0)

    def pack(slot, decay, end):
        packs[slot, 0:HV, :] = end.astype(jnp.bfloat16)
        packs[slot, HV:, :] = jnp.broadcast_to(decay, (16, n_key)).astype(jnp.bfloat16)

    def read(slot):
        return packs[slot, HV : HV + 1, :].astype(jnp.float32), packs[slot, 0:HV, :].astype(jnp.float32)

    def end_copy(source, target, number, place):
        return m.copy(packs.at[source], packs.at[target], end_send.at[number], end_recv.at[target], place)

    def join(early, late):
        return early[0] * late[0], early[1] * late[0] + late[1]

    def choose(flag, a, b):
        return jnp.where(flag, a[0], b[0]), jnp.where(flag, a[1], b[1])

    end_x = end_copy(0, 3, 0, m.other["x"])
    end_y = end_copy(1, 4, 1, m.other["y"])
    own_end = (jnp.exp(prefix[...]), state[...])
    pack(0, *own_end)

    arrived(pairs[0], m.piece(0))
    slab(acc2, w2, m.piece(0), True)
    end_x.start()
    pass_on(1, 2)
    enter(2)
    arrived(pairs[0], m.piece(1))
    slab(acc2, w2, m.piece(1), False)

    end_x.wait_recv()
    got = read(3)
    own_end = (jnp.exp(prefix[...]), state[...])
    none = (jnp.ones_like(got[0]), jnp.zeros_like(got[1]))
    late = x == 1
    pre = choose(late, got, none)
    two = choose(late, join(got, own_end), join(own_end, got))
    before[0:HV, :] = pre[1]
    before[HV:, :] = jnp.broadcast_to(pre[0], (8, n_key))
    pack(1, *two)
    pass_on(1, 3)
    arrived(pairs[0], m.piece(2))
    slab(acc2, w2, m.piece(2), False)
    end_y.start()
    arrived(pairs[0], m.piece(3))
    slab(acc2, w2, m.piece(3), False)
    end_y.wait_recv()
    got = read(4)
    two = read(1)
    pre = (before[HV : HV + 1, :], before[0:HV, :])
    late = y == 1
    pre = choose(late, join(got, pre), pre)
    four = choose(late, join(got, two), join(two, got))
    before[0:HV, :] = pre[1]
    before[HV:, :] = jnp.broadcast_to(pre[0], (8, n_key))
    pack(2, *four)

    pad = seq.shape[1] - rows

    def gate_tiles(low, high):
        def body(i, carry):
            at = pl.ds(pl.multiple_of(i * 128, 128), 128)
            for c in range(n_conv // 128):
                a = acc2[at, c * 128 : (c + 1) * 128].astype(jnp.bfloat16).astype(jnp.float32)
                g = acc2[at, n_conv + c * 128 : n_conv + (c + 1) * 128].astype(jnp.bfloat16).astype(jnp.float32)
                value = (a * jax.nn.sigmoid(g)).astype(jnp.bfloat16)
                seq[c, pl.ds(pl.multiple_of(i * 128 + pad, 32), 128), :] = value.astype(jnp.float32)
            return carry

        lax.fori_loop(low, high, body, 0)

    gate_tiles(rows // 128 - 1, rows // 128)
    for c in range(n_conv // 128):
        halo_out[:, c * 128 : (c + 1) * 128] = seq[c, rows : rows + pad, :].astype(jnp.bfloat16)
    gate_tiles(0, rows // 128 - 1)
    halo = m.copy(halo_out, halo_in, misc_send.at[1], misc_recv.at[1], me + 1)

    @pl.when(me < 15)
    def _():
        halo.start()

    for k in (1, 2, 3):
        @pl.when(z + k <= 3)
        def _():
            end_copy(2, 4 + k, 1 + k, me + 4 * k).start()

    n_taps = taps.shape[0]
    shift = pad - (n_taps - 1)

    def conv_chunk(i):
        base = pl.multiple_of(i * 128, 128)
        sums = jnp.zeros((128, 128), jnp.float32)
        squares = jnp.zeros((128, 128), jnp.float32)
        for c in range(n_conv // 128):
            part = seq[c, pl.ds(base, 128 + pad), :]
            total = jnp.zeros((128, 128), jnp.float32)
            for turn in range(8):
                moved = part if turn == 0 else pltpu.roll(part, 128 + pad - turn, 0)
                for tap in range(n_taps):
                    if (shift + tap) % 8 == turn:
                        start = shift + tap - turn
                        total = total + taps[tap : tap + 1, c * 128 : (c + 1) * 128] * moved[start : start + 128]
            acc2[pl.ds(base, 128), c * 128 : (c + 1) * 128] = total
            sums = sums + total
            squares = squares + total * total
        first = jnp.sum(sums, axis=1, keepdims=True)
        second = jnp.sum(squares, axis=1, keepdims=True)
        lane = lax.broadcasted_iota(jnp.int32, (128, 128), 1)
        stat_own[pl.ds(base, 128), :] = jnp.where(lane == 0, first, second)

    chunks = rows // 128

    def conv_loop(i, carry):
        conv_chunk(i)

        @pl.when(i == chunks // 2)
        def _():
            pass_on(2, 1)

        return carry

    lax.fori_loop(1, chunks, conv_loop, 0)

    @pl.when(me > 0)
    def _():
        halo.wait_recv()
        for c in range(n_conv // 128):
            seq[c, 0:pad, :] = halo_in[:, c * 128 : (c + 1) * 128].astype(jnp.float32)

    @pl.when(me == 0)
    def _():
        seq[:, 0:pad, :] = jnp.zeros((n_conv // 128, pad, 128), jnp.float32)

    lax.fori_loop(0, 1, conv_loop, 0)

    arrived(pairs[1], m.piece(0))
    slab(acc3, w3, m.piece(0), True)
    stats = m.copy(stat_own, stat_in, misc_send.at[2], misc_recv.at[2], me, 1 - tp)
    stats.start()
    arrived(pairs[1], m.piece(1))
    slab(acc3, w3, m.piece(1), False)
    pass_on(2, 2)
    arrived(pairs[1], m.piece(2))
    slab(acc3, w3, m.piece(2), False)
    arrived(pairs[1], m.piece(3))
    slab(acc3, w3, m.piece(3), False)

    stats.wait_recv()

    def conv_finish(i, carry):
        at = pl.ds(pl.multiple_of(i * 128, 128), 128)
        both_stats = stat_own[at, :] + stat_in[at, :]
        mean_val = both_stats[:, 0:1] / (2 * n_conv)
        square_mean = both_stats[:, 1:2] / (2 * n_conv)
        scale = lax.rsqrt(square_mean - mean_val * mean_val + epsilon)
        value = (acc2[at, 0:n_conv] - mean_val) * scale * conv_gain[...]
        act[at, 0:n_conv] = (value * jax.nn.sigmoid(value)).astype(jnp.bfloat16)
        return carry

    lax.fori_loop(0, chunks, conv_finish, 0)

    for k in (1, 2, 3):
        @pl.when(z - k >= 0)
        def _():
            end_copy(2, 4 + k, 1 + k, me).wait_recv()
            pre = join(read(4 + k), (before[HV : HV + 1, :], before[0:HV, :]))
            before[0:HV, :] = pre[1]
            before[HV:, :] = jnp.broadcast_to(pre[0], (8, n_key))

    state[...] = init[...] * before[HV : HV + 1, :] + before[0:HV, :]

    def gla_finish(i, carry):
        at = pl.ds(pl.multiple_of(i * 256, 256), 256)
        entering = state[...].astype(jnp.bfloat16)
        for h in range(heads):
            ks, vs = slice(h * HK, (h + 1) * HK), slice(h * HV, (h + 1) * HV)
            value = attn[at, vs] + dot(since[at, ks], entering[:, ks], ((1,), (1,)))
            value = value * lax.rsqrt(jnp.mean(value * value, axis=-1, keepdims=True) + epsilon) * head_gain[...]
            gate = acc3[at, vs].astype(jnp.bfloat16).astype(jnp.float32)
            act[at, n_conv + h * HV : n_conv + (h + 1) * HV] = (value * (gate * jax.nn.sigmoid(gate))).astype(jnp.bfloat16)
        return carry

    lax.fori_loop(0, rows // 256, gla_finish, 0)

    def part_copy(b):
        return m.copy(psend.at[b], precv.at[b], part_send.at[b], part_recv.at[b], me, 1 - tp)

    def out_block(p, yy):
        b = p * 2 + yy
        weight = jnp.concatenate([wo[p, yy, 0], wo[p, yy, 1]], axis=1)
        left = act[pl.ds(pl.multiple_of((1 - tp) * half, half), half), :]
        psend[b] = dot(left, weight, ((1,), (0,))).astype(jnp.bfloat16)
        left = act[pl.ds(pl.multiple_of(tp * half, half), half), :]
        pown[b] = dot(left, weight, ((1,), (0,))).astype(jnp.bfloat16)
        part_copy(b).start()

    def out_copy(b):
        return pltpu.make_async_copy(outv.at[b], out.at[:, pl.ds(pl.multiple_of(b * 256, 256), 256)], out_sem.at[b])

    def merge(p, yy):
        b = p * 2 + yy
        part_copy(b).wait_recv()
        outv[b] = (pown[b].astype(jnp.float32) + precv[b].astype(jnp.float32)).astype(jnp.bfloat16)
        out_copy(b).start()

    def out_pieces(j):
        def body(yy, carry):
            out_block(m.piece(j), yy)
            return carry

        arrived(pairs[2], m.piece(j))
        lax.fori_loop(0, 2, body, 0)

    def merges(j):
        def body(yy, carry):
            merge(m.piece(j), yy)
            return carry

        lax.fori_loop(0, 2, body, 0)

    out_pieces(0)
    out_pieces(1)
    merges(0)
    pass_on(2, 3)
    out_pieces(2)
    merges(1)
    out_pieces(3)
    merges(2)
    merges(3)

    swap.wait_send()
    stats.wait_send()

    @pl.when(me < 15)
    def _():
        halo.wait_send()

    end_x.wait_send()
    end_y.wait_send()
    for k in (1, 2, 3):
        @pl.when(z + k <= 3)
        def _():
            end_copy(2, 4 + k, 1 + k, me + 4 * k).wait_send()

    for p in range(4):
        for f in (b1, b2):
            f.first_copy(p).wait_send()
            f.last_copy(p).wait_send()
        for pair in pairs:
            for f in pair:
                f.last_copy(p).wait_send()
    for pair in pairs:
        for f in pair:
            f.first_copy(z).wait_send()
    whole.drain()
    for pair in lines:
        for line in pair:
            line.drain()
    for b in range(8):
        part_copy(b).wait_send()
        out_copy(b).wait()


def fused_layer(
    tokens, norm_gain, w_conv_a, w_conv_gate, conv_weight, conv_gain, w_query, w_key, w_value, w_outgate,
    w_decay, decay_bias, decay_extra, head_gain, init_state, w_out_conv, w_out_gla,
):
    rows, width = tokens.shape
    depth = w_query.shape[0]
    n_key = w_query.shape[1]
    n_conv = w_conv_a.shape[1]
    cols = w_out_conv.shape[1]
    init = init_state.transpose(2, 0, 1).reshape(HV, n_key)
    half = rows // 2
    pad = 32
    bf16, f32 = jnp.bfloat16, jnp.float32
    dma = pltpu.SemaphoreType.DMA
    vm = pl.BlockSpec(memory_space=pltpu.VMEM)
    hbm = pl.BlockSpec(memory_space=pl.ANY)
    return pl.pallas_call(
        layer_kernel,
        out_shape=jax.ShapeDtypeStruct((half, 2 * width), bf16),
        in_specs=[hbm, vm, hbm, hbm, vm, vm, hbm, hbm, hbm, hbm, hbm, vm, hbm, vm, vm, hbm, hbm],
        out_specs=hbm,
        scratch_shapes=[
            pltpu.VMEM((4, 2, 2, depth, 5 * n_key), bf16),
            pltpu.VMEM((4, 2, 2, depth, 2 * n_conv), bf16),
            pltpu.VMEM((4, 2, 2, depth, n_conv), bf16),
            pltpu.VMEM((4, 2, 2, 2 * n_conv, cols), bf16),
            pltpu.VMEM((2, rows, width), bf16),
            pltpu.VMEM((rows, 2 * width), bf16),
            pltpu.VMEM((rows, 5 * n_key), f32),
            pltpu.VMEM((rows, 2 * n_conv), f32),
            pltpu.VMEM((rows, n_conv), f32),
            pltpu.VMEM((rows, n_key), f32),
            pltpu.VMEM((n_conv // 128, rows + pad, 128), f32),
            pltpu.VMEM((rows, n_conv), f32),
            pltpu.VMEM((rows, n_key), bf16),
            pltpu.VMEM((rows, 2 * n_conv), bf16),
            pltpu.VMEM((8, half, 256), bf16),
            pltpu.VMEM((8, half, 256), bf16),
            pltpu.VMEM((8, half, 256), bf16),
            pltpu.VMEM((8, half, 256), bf16),
            pltpu.VMEM((pad, n_conv), bf16),
            pltpu.VMEM((pad, n_conv), bf16),
            pltpu.VMEM((rows, 128), f32),
            pltpu.VMEM((rows, 128), f32),
            pltpu.VMEM((8, HV + 16, n_key), bf16),
            pltpu.VMEM((HV, n_key), f32),
            pltpu.VMEM((1, n_key), f32),
            pltpu.VMEM((HV + 8, n_key), f32),
            dma((11,)), dma((8, 4)), dma((8, 4)), dma((8, 4)), dma((8, 4)), dma((7, 4)), dma((7, 4)), dma((7, 4)),
            dma((3,)), dma((3,)), dma((5,)), dma((8,)), dma((8,)), dma((8,)), dma((8,)),
        ],
        compiler_params=pltpu.CompilerParams(collective_id=0, has_side_effects=True, vmem_limit_bytes=67043328),
        name="layer",
    )(
        tokens, norm_gain[None, :], w_conv_a, w_conv_gate, conv_weight, conv_gain[None, :], w_query, w_key, w_value,
        w_outgate, w_decay, decay_bias[None, :], decay_extra, head_gain[None, :], init, w_out_conv, w_out_gla,
    )


def local_kernel(heads, pieces, q_ref, k_ref, v_ref, pre_ref, extra_ref, bias_ref, attn_ref, since_ref, end_ref, log_ref, state, prefix):
    step = pl.program_id(0)

    @pl.when(step == 0)
    def _():
        state[...] = jnp.zeros_like(state)
        prefix[...] = jnp.zeros_like(prefix)

    rows = lax.broadcasted_iota(jnp.int32, (BLOCK, BLOCK), 0)
    columns = lax.broadcasted_iota(jnp.int32, (BLOCK, BLOCK), 1)
    causal = rows >= columns
    lower = causal.astype(jnp.float32)
    for piece in range(pieces):
        at = pl.ds(piece * BLOCK, BLOCK)
        pre = pre_ref[at, :] + bias_ref[...]
        logs = jax.nn.log_sigmoid(pre) / gate_divisor + extra_ref[at, :]
        cum = lax.dot_general(
            lower, logs, (((1,), (0,)), ((), ())), precision=lax.Precision.HIGHEST, preferred_element_type=jnp.float32
        )
        total = cum[BLOCK - 1 :, :]
        middle = cum[BLOCK // 2 - 1 : BLOCK // 2, :]
        query = q_ref[at, :].astype(jnp.float32) * HK ** (-0.5)
        keys = k_ref[at, :].astype(jnp.float32)
        decayed = query * jnp.exp(cum)
        since_ref[at, :] = (decayed * jnp.exp(prefix[...])).astype(jnp.bfloat16)
        decayed = decayed.astype(jnp.bfloat16)
        query = (query * jnp.exp(cum - middle)).astype(jnp.bfloat16)
        inverse = (keys * jnp.exp(middle - cum)).astype(jnp.bfloat16)
        to_end = (keys * jnp.exp(total - cum)).astype(jnp.bfloat16)
        entering = state[...].astype(jnp.bfloat16)
        added = []
        for h in range(heads):
            ks, vs = slice(h * HK, (h + 1) * HK), slice(h * HV, (h + 1) * HV)
            values = v_ref[at, vs]
            scores = jnp.where(causal, dot(query[:, ks], inverse[:, ks], ((1,), (1,))), 0.0)
            attn_ref[at, vs] = dot(scores.astype(jnp.bfloat16), values, ((1,), (0,))) + dot(
                decayed[:, ks], entering[:, ks], ((1,), (1,))
            )
            added.append(dot(values, to_end[:, ks], ((0,), (0,))))
        added = added[0] if heads == 1 else jnp.concatenate(added, axis=1)
        state[...] = state[...] * jnp.exp(total) + added
        prefix[...] = prefix[...] + total
    end_ref[...] = state[...]
    log_ref[...] = prefix[...]


def gla_local(query, keys, values, decay_pre, decay_extra, decay_bias):
    rows, width = query.shape
    heads = width // HK
    pieces = 4
    tile = pieces * BLOCK

    def tiled(array):
        return pl.BlockSpec((tile, array.shape[1]), lambda i: (i, 0))

    def whole(shape):
        return pl.BlockSpec(shape, lambda i: (0, 0))

    return pl.pallas_call(
        functools.partial(local_kernel, heads, pieces),
        grid=(rows // tile,),
        in_specs=[tiled(query), tiled(keys), tiled(values), tiled(decay_pre), tiled(decay_extra), whole((1, width))],
        out_specs=[tiled(values), tiled(query), whole((HV, width)), whole((1, width))],
        out_shape=[
            jax.ShapeDtypeStruct(values.shape, jnp.float32),
            jax.ShapeDtypeStruct(query.shape, jnp.bfloat16),
            jax.ShapeDtypeStruct((HV, width), jnp.float32),
            jax.ShapeDtypeStruct((1, width), jnp.float32),
        ],
        scratch_shapes=[pltpu.VMEM((HV, width), jnp.float32), pltpu.VMEM((1, width), jnp.float32)],
        cost_estimate=pl.CostEstimate(flops=10**10, bytes_accessed=10**7, transcendentals=10**6),
        name="gla_local",
    )(query, keys, values, decay_pre, decay_extra, decay_bias[None, :])


def finish_kernel(heads, size, where_ref, attn_ref, since_ref, gate_ref, ends_ref, init_ref, gain_ref, out_ref, state):
    me = where_ref[0]

    @pl.when(pl.program_id(0) == 0)
    def _():
        state[...] = init_ref[...]

        def one(device, carry):
            at = device
            decay = ends_ref[pl.ds(pl.multiple_of(at * size + HV, 16), 16), :].astype(jnp.float32)[:1]
            end = ends_ref[pl.ds(pl.multiple_of(at * size, 16), HV), :].astype(jnp.float32)
            state[...] = state[...] * decay + end
            return carry

        lax.fori_loop(0, me, one, 0)

    entering = state[...].astype(jnp.bfloat16)
    for h in range(heads):
        ks, vs = slice(h * HK, (h + 1) * HK), slice(h * HV, (h + 1) * HV)
        attn = attn_ref[:, vs] + dot(since_ref[:, ks], entering[:, ks], ((1,), (1,)))
        attn = attn * lax.rsqrt(jnp.mean(attn * attn, axis=-1, keepdims=True) + epsilon) * gain_ref[...]
        gate = gate_ref[:, vs].astype(jnp.float32)
        out_ref[:, vs] = (attn * (gate * jax.nn.sigmoid(gate))).astype(jnp.bfloat16)


def gla_finish(attn, since, out_gate, ends, init_state, head_gain, me):
    rows, width = since.shape
    heads = width // HK
    tile = 256

    def tiled(array):
        return pl.BlockSpec((tile, array.shape[1]), lambda i, w: (i, 0))

    def whole(array):
        return pl.BlockSpec(array.shape, lambda i, w: (0, 0))

    init = init_state.transpose(2, 0, 1).reshape(HV, width)
    gain = head_gain[None, :]
    return pl.pallas_call(
        functools.partial(finish_kernel, heads, HV + 16),
        grid_spec=pltpu.PrefetchScalarGridSpec(
            num_scalar_prefetch=1,
            grid=(rows // tile,),
            in_specs=[tiled(attn), tiled(since), tiled(out_gate), whole(ends), whole(init), whole(gain)],
            out_specs=tiled(attn),
            scratch_shapes=[pltpu.VMEM((HV, width), jnp.float32)],
        ),
        out_shape=jax.ShapeDtypeStruct(attn.shape, jnp.bfloat16),
        cost_estimate=pl.CostEstimate(flops=3 * 10**9, bytes_accessed=10**7, transcendentals=10**6),
        name="gla_finish",
    )(me[None], attn, since, out_gate, ends, init, gain)


def conv_branch(gated, conv_weight, conv_gain):
    taps = conv_weight.shape[0]
    row_count = gated.shape[0]
    count = lax.axis_size("sp")
    earlier = lax.ppermute(gated[row_count - taps + 1 :], "sp", [(i, i + 1) for i in range(count - 1)])
    extended = jnp.concatenate([earlier, gated], axis=0).astype(jnp.float32)
    conv_sum = jnp.zeros(gated.shape, jnp.float32)
    for tap in range(taps):
        conv_sum = conv_sum + conv_weight[tap][None, :] * extended[tap : tap + row_count]
    row_sums, row_squares = lax.psum((jnp.sum(conv_sum, axis=1), jnp.sum(conv_sum * conv_sum, axis=1)), "tp")
    mean_val = (row_sums / D_CONV)[:, None]
    square_mean = (row_squares / D_CONV)[:, None]
    conv_norm = (conv_sum - mean_val) * lax.rsqrt(square_mean - mean_val * mean_val + epsilon) * conv_gain
    return jax.nn.silu(conv_norm).astype(jnp.bfloat16)


def project(hidden, weight):
    return dot(hidden, weight, ((1,), (0,)))


def plain_layer(
    tokens, norm_gain, w_conv_a, w_conv_gate, conv_weight, conv_gain, w_query, w_key, w_value, w_outgate,
    w_decay, decay_bias, decay_extra, head_gain, init_state, w_out_conv, w_out_gla,
):
    me = lax.axis_index("sp")

    def gather(shard):
        return lax.all_gather(shard, "sp", axis=0, tiled=True)

    widened = lax.all_gather(tokens, "tp", axis=1, tiled=True).astype(jnp.float32)
    normed = (
        widened * lax.rsqrt(jnp.mean(widened * widened, axis=-1, keepdims=True) + epsilon) * norm_gain
    ).astype(jnp.bfloat16)
    half = w_query.shape[1]
    conv_a = project(normed, gather(w_conv_a)).astype(jnp.bfloat16)
    conv_gate = project(normed, gather(w_conv_gate)).astype(jnp.bfloat16)
    full_qkd = gather(jnp.concatenate([w_query, w_key, w_decay], axis=1))
    full_v = gather(w_value)
    gated = (conv_a.astype(jnp.float32) * jax.nn.sigmoid(conv_gate.astype(jnp.float32))).astype(jnp.bfloat16)
    conv_out = conv_branch(gated, conv_weight, conv_gain)
    query_keys = project(normed, full_qkd[:, : 2 * half]).astype(jnp.bfloat16)
    decay_pre = project(normed, full_qkd[:, 2 * half :])
    values = project(normed, full_v).astype(jnp.bfloat16)
    attn, since, end, end_log = gla_local(
        query_keys[:, :half], query_keys[:, half:], values, decay_pre, decay_extra, decay_bias
    )
    packed = jnp.concatenate([end, jnp.broadcast_to(jnp.exp(end_log), (16, half))], axis=0).astype(jnp.bfloat16)
    ends = gather(packed)
    out_gate = project(normed, gather(w_outgate)).astype(jnp.bfloat16)
    gla_out = gla_finish(attn, since, out_gate, ends, init_state, head_gain, me)
    total = dot(conv_out, gather(w_out_conv.T), ((1,), (1,))) + dot(gla_out, gather(w_out_gla.T), ((1,), (1,)))
    return lax.psum_scatter(total.astype(jnp.bfloat16), "tp", scatter_dimension=0, tiled=True)


def per_device(*arrays):
    if folded(lax.axis_size("sp"), lax.axis_size("tp")):
        return fused_layer(*arrays)
    return plain_layer(*arrays)


def solution(mesh):
    placed = (
        P("sp", "tp"), P(), P("sp", "tp"), P("sp", "tp"), P(None, "tp"), P("tp"), P("sp", "tp"), P("sp", "tp"),
        P("sp", "tp"), P("sp", "tp"), P("sp", "tp"), P("tp"), P("sp", "tp"), P(), P("tp", None, None),
        P("tp", "sp"), P("tp", "sp"),
    )
    return jax.shard_map(
        per_device, mesh=mesh, in_specs=placed, out_specs=P(("sp", "tp"), None), check_vma=False
    )
```

profile of v0, /device:TPU:25, one launch (start us, length us, event | category | flops | bytes accessed | tf_op | source)
XLA Modules:
  0.0 151.4 jit_solution(17321477897361091880)
XLA Ops:
  0.0 1.7 %copy.19.init = f32[128,256]{1,0:T(8,128)} copy(f32[128,256]{0,1:T(8,128)} %bitcast.7) | data formatting | bytes 262144 | tf_op jit(solution)/shard_map/reshape | solution.py:639
  1.7 146.6 %layer.1 = bf16[512,2048]{1,0:T(8,128)(2,1)} custom-call(bf16[1024,1024]{1,0:T(8,128)(2,1)} %tokens.1, f32[1,2048]{1,0:T(1,128)} %bitcast.8, bf16[128,512]{1,0:T(8,128)(2,1)} %wa.1, bf16[128,512]{1,0:T(8,128)(2,1)} %wg.1, f32[31,512]{1,0:T(8,128)} %taps.1, f32[1,512]{1,0:T(1,128)} %bitcast.9, bf16[128,256]{1,0:T(8,128)(2,1)} %wq.1, bf16[128,256]{1,0:T(8,128)(2,1)} %wk.1, ...), custom_call_target="tpu_custom_call" | custom-call | tf_op jit(solution)/shard_map/layer/pallas_call | solution.py:646
  148.3 3.2 %copy.21 = bf16[512,2048]{1,0:T(8,128)(2,1)} copy(bf16[512,2048]{1,0:T(8,128)(2,1)} %layer.1) | data formatting | bytes 4194304
where the time goes:
time: 152 us; the launch traced here: 151 us
  Pallas kernels  147 us (97%)
  local copies, waits for them, and re-layouts  4.82 us (3%)
    pallas_call x1, Pallas kernels, fused_layer(): pl.pallas_call(layer_kernel, out_shape=jax.ShapeDtypeStruct((half, 2 * wi...  147 us
    unnamed x1, local copies, waits for them, and re-layouts  3.16 us

commit v1 on v0

--- a/solution.py
+++ b/solution.py
@@ -179,7 +179,8 @@
     pairs = [
         (Flow(m, 2, lanes(w2, 0, n_conv), "x", sems), Flow(m, 3, lanes(w2, n_conv, n_conv), "y", sems)),
         (Flow(m, 4, lanes(w3, 0, n_key), "x", sems), Flow(m, 5, lanes(w3, n_key, n_key), "y", sems)),
-        (Flow(m, 6, depth(0, n_conv), "x", sems), Flow(m, 7, depth(n_conv, n_conv), "y", sems)),
+        (Flow(m, 6, depth(0, n_key), "x", sems), Flow(m, 7, depth(n_key, n_key), "y", sems)),
+        (Flow(m, 8, depth(n_conv, n_key), "x", sems), Flow(m, 9, depth(n_conv + n_key, n_key), "y", sems)),
     ]
     whole = Line(m, 0, lambda p: w1.at[p, y, x], sems)
     lines = [tuple(Line(m, f.number - 1, f.pair, sems) for f in pair) for pair in pairs]
@@ -220,12 +221,11 @@
     loads[5].wait()
     for f in pairs[0]:
         f.first_copy(z).start()
-    for i in (6, 7, 8):
+    loads[6].wait()
+    for f in pairs[1]:
+        f.first_copy(z).start()
+    for i in (7, 8, 10):
         loads[i].wait()
-    for pair in pairs[1:]:
-        for f in pair:
-            f.first_copy(z).start()
-    loads[10].wait()
 
     def head_firsts(step):
         def one(p):
@@ -243,10 +243,17 @@
 
         whole.relay(step, then)
 
+    def begin(k):
+        for f in pairs[k]:
+            f.first_copy(z).start()
+
     def enter(k):
         for f, line in zip(pairs[k], lines[k]):
             f.first_copy(z).wait_recv()
             line.start_own()
+
+    def own_last(k):
+        for f in pairs[k]:
             f.last_copy(z).start()
 
     def pass_on(k, step):
@@ -295,17 +302,22 @@
     enter(0)
     head_firsts(1)
     head_line(3)
-    head_firsts(2)
     arrived((b1, b2), m.piece(0))
     slab(acc1, w1, m.piece(0), True)
-    head_firsts(3)
+    head_firsts(2)
+    begin(2)
+    begin(3)
+    pass_on(0, 1)
     arrived((b1, b2), m.piece(1))
     slab(acc1, w1, m.piece(1), False)
-    pass_on(0, 1)
+    head_firsts(3)
+    enter(1)
+    own_last(0)
+    pass_on(0, 2)
     arrived((b1, b2), m.piece(2))
     slab(acc1, w1, m.piece(2), False)
-    pass_on(0, 2)
-    enter(1)
+    pass_on(1, 1)
+    enter(2)
     arrived((b1, b2), m.piece(3))
     slab(acc1, w1, m.piece(3), False)
 
@@ -348,18 +360,18 @@
         return carry
 
     blocks = rows // BLOCK
-    quarter = blocks // 4
 
     def attend(i, carry):
         block(i, 0)
 
-        @pl.when(i == quarter)
+        @pl.when(i == blocks // 2)
         def _():
+            own_last(1)
             pass_on(0, 3)
 
-        @pl.when(i == 3 * quarter)
+        @pl.when(i == blocks - 3)
         def _():
-            pass_on(1, 1)
+            pass_on(1, 2)
 
         return carry
 
@@ -389,37 +401,38 @@
     arrived(pairs[0], m.piece(0))
     slab(acc2, w2, m.piece(0), True)
     end_x.start()
-    pass_on(1, 2)
-    enter(2)
+    pass_on(2, 1)
+    enter(3)
     arrived(pairs[0], m.piece(1))
     slab(acc2, w2, m.piece(1), False)
-
-    end_x.wait_recv()
-    got = read(3)
-    own_end = (jnp.exp(prefix[...]), state[...])
-    none = (jnp.ones_like(got[0]), jnp.zeros_like(got[1]))
-    late = x == 1
-    pre = choose(late, got, none)
-    two = choose(late, join(got, own_end), join(own_end, got))
-    before[0:HV, :] = pre[1]
-    before[HV:, :] = jnp.broadcast_to(pre[0], (8, n_key))
-    pack(1, *two)
-    pass_on(1, 3)
     arrived(pairs[0], m.piece(2))
     slab(acc2, w2, m.piece(2), False)
-    end_y.start()
     arrived(pairs[0], m.piece(3))
     slab(acc2, w2, m.piece(3), False)
-    end_y.wait_recv()
-    got = read(4)
-    two = read(1)
-    pre = (before[HV : HV + 1, :], before[0:HV, :])
-    late = y == 1
-    pre = choose(late, join(got, pre), pre)
-    four = choose(late, join(got, two), join(two, got))
-    before[0:HV, :] = pre[1]
-    before[HV:, :] = jnp.broadcast_to(pre[0], (8, n_key))
-    pack(2, *four)
+    pass_on(1, 3)
+    own_last(2)
+
+    def join_x():
+        end_x.wait_recv()
+        got = read(3)
+        own = (jnp.exp(prefix[...]), state[...])
+        none = (jnp.ones_like(got[0]), jnp.zeros_like(got[1]))
+        late = x == 1
+        pre = choose(late, got, none)
+        before[0:HV, :] = pre[1]
+        before[HV:, :] = jnp.broadcast_to(pre[0], (8, n_key))
+        pack(1, *choose(late, join(got, own), join(own, got)))
+
+    def join_y():
+        end_y.wait_recv()
+        got = read(4)
+        two = read(1)
+        pre = (before[HV : HV + 1, :], before[0:HV, :])
+        late = y == 1
+        pre = choose(late, join(got, pre), pre)
+        before[0:HV, :] = pre[1]
+        before[HV:, :] = jnp.broadcast_to(pre[0], (8, n_key))
+        pack(2, *choose(late, join(got, two), join(two, got)))
 
     pad = seq.shape[1] - rows
 
@@ -445,11 +458,7 @@
     def _():
         halo.start()
 
-    for k in (1, 2, 3):
-        @pl.when(z + k <= 3)
-        def _():
-            end_copy(2, 4 + k, 1 + k, me + 4 * k).start()
-
+    join_x()
     n_taps = taps.shape[0]
     shift = pad - (n_taps - 1)
 
@@ -481,7 +490,8 @@
 
         @pl.when(i == chunks // 2)
         def _():
-            pass_on(2, 1)
+            end_y.start()
+            pass_on(2, 2)
 
         return carry
 
@@ -499,17 +509,25 @@
 
     lax.fori_loop(0, 1, conv_loop, 0)
 
+    pass_on(3, 1)
+    own_last(3)
     arrived(pairs[1], m.piece(0))
     slab(acc3, w3, m.piece(0), True)
     stats = m.copy(stat_own, stat_in, misc_send.at[2], misc_recv.at[2], me, 1 - tp)
     stats.start()
+    join_y()
     arrived(pairs[1], m.piece(1))
     slab(acc3, w3, m.piece(1), False)
-    pass_on(2, 2)
+    for k in (1, 2, 3):
+        @pl.when(z + k <= 3)
+        def _():
+            end_copy(2, 4 + k, 1 + k, me + 4 * k).start()
+
     arrived(pairs[1], m.piece(2))
     slab(acc3, w3, m.piece(2), False)
     arrived(pairs[1], m.piece(3))
     slab(acc3, w3, m.piece(3), False)
+    pass_on(2, 3)
 
     stats.wait_recv()
 
@@ -533,7 +551,8 @@
             before[0:HV, :] = pre[1]
             before[HV:, :] = jnp.broadcast_to(pre[0], (8, n_key))
 
-    state[...] = init[...] * before[HV : HV + 1, :] + before[0:HV, :]
+    entry = jnp.concatenate([init[h].T for h in range(heads)], axis=1)
+    state[...] = entry * before[HV : HV + 1, :] + before[0:HV, :]
 
     def gla_finish(i, carry):
         at = pl.ds(pl.multiple_of(i * 256, 256), 256)
@@ -574,7 +593,7 @@
             out_block(m.piece(j), yy)
             return carry
 
-        arrived(pairs[2], m.piece(j))
+        arrived(pairs[2] + pairs[3], m.piece(j))
         lax.fori_loop(0, 2, body, 0)
 
     def merges(j):
@@ -587,11 +606,12 @@
     out_pieces(0)
     out_pieces(1)
     merges(0)
-    pass_on(2, 3)
+    pass_on(3, 2)
     out_pieces(2)
     merges(1)
+    pass_on(3, 3)
+    merges(2)
     out_pieces(3)
-    merges(2)
     merges(3)
 
     swap.wait_send()
@@ -636,7 +656,6 @@
     n_key = w_query.shape[1]
     n_conv = w_conv_a.shape[1]
     cols = w_out_conv.shape[1]
-    init = init_state.transpose(2, 0, 1).reshape(HV, n_key)
     half = rows // 2
     pad = 32
     bf16, f32 = jnp.bfloat16, jnp.float32
@@ -675,14 +694,14 @@
             pltpu.VMEM((HV, n_key), f32),
             pltpu.VMEM((1, n_key), f32),
             pltpu.VMEM((HV + 8, n_key), f32),
-            dma((11,)), dma((8, 4)), dma((8, 4)), dma((8, 4)), dma((8, 4)), dma((7, 4)), dma((7, 4)), dma((7, 4)),
+            dma((11,)), dma((10, 4)), dma((10, 4)), dma((10, 4)), dma((10, 4)), dma((9, 4)), dma((9, 4)), dma((9, 4)),
             dma((3,)), dma((3,)), dma((5,)), dma((8,)), dma((8,)), dma((8,)), dma((8,)),
         ],
         compiler_params=pltpu.CompilerParams(collective_id=0, has_side_effects=True, vmem_limit_bytes=67043328),
         name="layer",
     )(
         tokens, norm_gain[None, :], w_conv_a, w_conv_gate, conv_weight, conv_gain[None, :], w_query, w_key, w_value,
-        w_outgate, w_decay, decay_bias[None, :], decay_extra, head_gain[None, :], init, w_out_conv, w_out_gla,
+        w_outgate, w_decay, decay_bias[None, :], decay_extra, head_gain[None, :], init_state, w_out_conv, w_out_gla,
     )
 
 

time: 152 us -> 139 us (0.914)
  Pallas kernels: 147 us -> 136 us
  local copies, waits for them, and re-layouts: 4.82 us -> 3.16 us
    pallas_call x1, Pallas kernels: 147 us -> 136 us  [fused_layer(): pl.pallas_call(layer_kernel, out_shape=jax.ShapeDtypeStruct((half, 2 * wi...]
    reshape x1 -> x0, local copies, waits for them, and re-layouts: 1.66 us -> none  [fused_layer(): init = init_state.transpose(2, 0, 1).reshape(HV, n_key)]
where the time goes in v1:
time: 139 us
  Pallas kernels  136 us (98%)
  local copies, waits for them, and re-layouts  3.16 us (2%)
    pallas_call x1, Pallas kernels, fused_layer(): pl.pallas_call(layer_kernel, out_shape=jax.ShapeDtypeStruct((half, 2 * wi...  136 us
    unnamed x1, local copies, waits for them, and re-layouts  3.16 us

profile of v1, /device:TPU:25, one launch (start us, length us, event | category | flops | bytes accessed | tf_op | source)
XLA Modules:
  0.0 138.8 jit_solution(8693746579066590365)
XLA Ops:
  0.0 135.7 %layer.1 = bf16[512,2048]{1,0:T(8,128)(2,1)} custom-call(bf16[1024,1024]{1,0:T(8,128)(2,1)} %tokens.1, f32[1,2048]{1,0:T(1,128)} %bitcast.4, bf16[128,512]{1,0:T(8,128)(2,1)} %wa.1, bf16[128,512]{1,0:T(8,128)(2,1)} %wg.1, f32[31,512]{1,0:T(8,128)} %taps.1, f32[1,512]{1,0:T(1,128)} %bitcast.5, bf16[128,256]{1,0:T(8,128)(2,1)} %wq.1, bf16[128,256]{1,0:T(8,128)(2,1)} %wk.1, ...), custom_call_target="tpu_custom_call" | custom-call | tf_op jit(solution)/shard_map/layer/pallas_call | solution.py:665
  135.7 3.2 %copy.19 = bf16[512,2048]{1,0:T(8,128)(2,1)} copy(bf16[512,2048]{1,0:T(8,128)(2,1)} %layer.1) | data formatting | bytes 4194304

commit v2 on v1

--- a/solution.py
+++ b/solution.py
@@ -32,6 +32,7 @@
         self.tp = lax.axis_index("tp")
         self.z, self.y, self.x = self.me // 4, (self.me // 2) % 2, self.me % 2
         self.other = {"x": self.me + 1 - 2 * self.x, "y": self.me + 2 - 4 * self.y}
+        self.across = self.me + 3 - 2 * self.x - 4 * self.y
         self.sent = []
 
     def copy(self, source, target, send, recv, place, core=None):
@@ -148,11 +149,11 @@
 
 
 def layer_kernel(
-    tokens, gain, wa, wg, taps, conv_gain, wq, wk, wv, wog, wd, bias, extra_in, head_gain, init, woc, wogl, out,
-    w1, w2, w3, wo, both, normed, acc1, acc2, acc3, extra, seq, attn, since, act, psend, pown, precv, outv,
+    tokens, gain, wa, wg, taps, conv_gain, wq, wk, wv, wog, wd, bias, extra_in, head_gain, init, woc, wogl, own_out, other_out,
+    w1, w2, w3, wo, both, normed, acc1, acc2, acc3, extra, seq, attn, since, act, psend,
     halo_out, halo_in, stat_own, stat_in, packs, state, prefix, before,
     local, first_send, first_recv, last_send, last_recv, up_send, down_send, z_recv, misc_send, misc_recv, end_send, end_recv,
-    part_send, part_recv, out_sem,
+    part_send, part_recv,
 ):
     m = Mover()
     me, tp, z, y, x = m.me, m.tp, m.z, m.y, m.x
@@ -174,13 +175,15 @@
         return lambda p, yy, xx: wo.at[p, yy, xx, pl.ds(low, size), :]
 
     mid = w1.shape[-1] // 2
+    late = wo.shape[3] // 8
+    early = wo.shape[3] // 2 - late
     b1 = Flow(m, 0, lanes(w1, 0, mid), "x", sems)
     b2 = Flow(m, 1, lanes(w1, mid, mid), "y", sems)
     pairs = [
         (Flow(m, 2, lanes(w2, 0, n_conv), "x", sems), Flow(m, 3, lanes(w2, n_conv, n_conv), "y", sems)),
         (Flow(m, 4, lanes(w3, 0, n_key), "x", sems), Flow(m, 5, lanes(w3, n_key, n_key), "y", sems)),
-        (Flow(m, 6, depth(0, n_key), "x", sems), Flow(m, 7, depth(n_key, n_key), "y", sems)),
-        (Flow(m, 8, depth(n_conv, n_key), "x", sems), Flow(m, 9, depth(n_conv + n_key, n_key), "y", sems)),
+        (Flow(m, 6, depth(0, early), "x", sems), Flow(m, 7, depth(early, early), "y", sems)),
+        (Flow(m, 8, depth(2 * early, late), "x", sems), Flow(m, 9, depth(2 * early + late, late), "y", sems)),
     ]
     whole = Line(m, 0, lambda p: w1.at[p, y, x], sems)
     lines = [tuple(Line(m, f.number - 1, f.pair, sems) for f in pair) for pair in pairs]
@@ -203,7 +206,7 @@
         load.start()
 
     barrier = pltpu.get_barrier_semaphore()
-    partners = [(m.other["x"], tp), (m.other["y"], tp), (me, 1 - tp)]
+    partners = [(m.other["x"], tp), (m.other["y"], tp), (m.across, tp), (me, 1 - tp)]
     partners += [((me + k) % 16, tp) for k in (4, 8, 12, 1, 15)]
     for place, core in partners:
         pl.semaphore_signal(barrier, inc=1, device_id=(place, core), device_id_type=MESH)
@@ -247,10 +250,13 @@
         for f in pairs[k]:
             f.first_copy(z).start()
 
+    def enter_one(k, i):
+        pairs[k][i].first_copy(z).wait_recv()
+        lines[k][i].start_own()
+
     def enter(k):
-        for f, line in zip(pairs[k], lines[k]):
-            f.first_copy(z).wait_recv()
-            line.start_own()
+        enter_one(k, 0)
+        enter_one(k, 1)
 
     def own_last(k):
         for f in pairs[k]:
@@ -298,8 +304,9 @@
     head_line(1)
     head_firsts(0)
     norm_tiles(4, 8)
+    enter_one(0, 0)
     head_line(2)
-    enter(0)
+    enter_one(0, 1)
     head_firsts(1)
     head_line(3)
     arrived((b1, b2), m.piece(0))
@@ -390,17 +397,17 @@
     def join(early, late):
         return early[0] * late[0], early[1] * late[0] + late[1]
 
-    def choose(flag, a, b):
-        return jnp.where(flag, a[0], b[0]), jnp.where(flag, a[1], b[1])
-
-    end_x = end_copy(0, 3, 0, m.other["x"])
-    end_y = end_copy(1, 4, 1, m.other["y"])
-    own_end = (jnp.exp(prefix[...]), state[...])
-    pack(0, *own_end)
+    near_ends = [
+        end_copy(0, 1, 0, m.other["x"]),
+        end_copy(0, 2, 1, m.other["y"]),
+        end_copy(0, 3, 2, m.across),
+    ]
+    pack(0, jnp.exp(prefix[...]), state[...])
 
     arrived(pairs[0], m.piece(0))
     slab(acc2, w2, m.piece(0), True)
-    end_x.start()
+    for end in near_ends:
+        end.start()
     pass_on(2, 1)
     enter(3)
     arrived(pairs[0], m.piece(1))
@@ -412,27 +419,22 @@
     pass_on(1, 3)
     own_last(2)
 
-    def join_x():
-        end_x.wait_recv()
-        got = read(3)
-        own = (jnp.exp(prefix[...]), state[...])
-        none = (jnp.ones_like(got[0]), jnp.zeros_like(got[1]))
-        late = x == 1
-        pre = choose(late, got, none)
+    def join_near():
+        for end in near_ends:
+            end.wait_recv()
+        run = (jnp.ones((1, n_key), jnp.float32), jnp.zeros((HV, n_key), jnp.float32))
+        pre = run
+        for yy in range(2):
+            for xx in range(2):
+                past = yy * 2 + xx < y * 2 + x
+                run = join(run, read((y + yy - 2 * y * yy) * 2 + x + xx - 2 * x * xx))
+                pre = jnp.where(past, run[0], pre[0]), jnp.where(past, run[1], pre[1])
         before[0:HV, :] = pre[1]
         before[HV:, :] = jnp.broadcast_to(pre[0], (8, n_key))
-        pack(1, *choose(late, join(got, own), join(own, got)))
-
-    def join_y():
-        end_y.wait_recv()
-        got = read(4)
-        two = read(1)
-        pre = (before[HV : HV + 1, :], before[0:HV, :])
-        late = y == 1
-        pre = choose(late, join(got, pre), pre)
-        before[0:HV, :] = pre[1]
-        before[HV:, :] = jnp.broadcast_to(pre[0], (8, n_key))
-        pack(2, *choose(late, join(got, two), join(two, got)))
+        pack(4, *run)
+
+    def far_end(k):
+        return end_copy(4, 4 + k, 2 + k, me + 4 * k)
 
     pad = seq.shape[1] - rows
 
@@ -458,7 +460,6 @@
     def _():
         halo.start()
 
-    join_x()
     n_taps = taps.shape[0]
     shift = pad - (n_taps - 1)
 
@@ -490,7 +491,6 @@
 
         @pl.when(i == chunks // 2)
         def _():
-            end_y.start()
             pass_on(2, 2)
 
         return carry
@@ -515,20 +515,19 @@
     slab(acc3, w3, m.piece(0), True)
     stats = m.copy(stat_own, stat_in, misc_send.at[2], misc_recv.at[2], me, 1 - tp)
     stats.start()
-    join_y()
+    join_near()
     arrived(pairs[1], m.piece(1))
     slab(acc3, w3, m.piece(1), False)
     for k in (1, 2, 3):
         @pl.when(z + k <= 3)
         def _():
-            end_copy(2, 4 + k, 1 + k, me + 4 * k).start()
+            far_end(k).start()
 
     arrived(pairs[1], m.piece(2))
     slab(acc3, w3, m.piece(2), False)
     arrived(pairs[1], m.piece(3))
     slab(acc3, w3, m.piece(3), False)
     pass_on(2, 3)
-
     stats.wait_recv()
 
     def conv_finish(i, carry):
@@ -542,11 +541,11 @@
         return carry
 
     lax.fori_loop(0, chunks, conv_finish, 0)
-
+    pass_on(3, 2)
     for k in (1, 2, 3):
         @pl.when(z - k >= 0)
         def _():
-            end_copy(2, 4 + k, 1 + k, me).wait_recv()
+            end_copy(4, 4 + k, 2 + k, me).wait_recv()
             pre = join(read(4 + k), (before[HV : HV + 1, :], before[0:HV, :]))
             before[0:HV, :] = pre[1]
             before[HV:, :] = jnp.broadcast_to(pre[0], (8, n_key))
@@ -568,83 +567,116 @@
     lax.fori_loop(0, rows // 256, gla_finish, 0)
 
     def part_copy(b):
-        return m.copy(psend.at[b], precv.at[b], part_send.at[b], part_recv.at[b], me, 1 - tp)
-
-    def out_block(p, yy):
-        b = p * 2 + yy
+        at = pl.ds(pl.multiple_of(b * 256, 256), 256)
+        return m.copy(psend.at[b], other_out.at[:, at], part_send.at[b], part_recv.at[b], me, 1 - tp)
+
+    def project(p, yy, core):
         weight = jnp.concatenate([wo[p, yy, 0], wo[p, yy, 1]], axis=1)
-        left = act[pl.ds(pl.multiple_of((1 - tp) * half, half), half), :]
-        psend[b] = dot(left, weight, ((1,), (0,))).astype(jnp.bfloat16)
-        left = act[pl.ds(pl.multiple_of(tp * half, half), half), :]
-        pown[b] = dot(left, weight, ((1,), (0,))).astype(jnp.bfloat16)
-        part_copy(b).start()
-
-    def out_copy(b):
-        return pltpu.make_async_copy(outv.at[b], out.at[:, pl.ds(pl.multiple_of(b * 256, 256), 256)], out_sem.at[b])
-
-    def merge(p, yy):
-        b = p * 2 + yy
-        part_copy(b).wait_recv()
-        outv[b] = (pown[b].astype(jnp.float32) + precv[b].astype(jnp.float32)).astype(jnp.bfloat16)
-        out_copy(b).start()
+        left = act[pl.ds(pl.multiple_of(core * half, half), half), :]
+        return dot(left, weight, ((1,), (0,))).astype(jnp.bfloat16)
 
     def out_pieces(j):
+        p = m.piece(j)
+
+        def theirs(yy, carry):
+            psend[p * 2 + yy] = project(p, yy, 1 - tp)
+            return carry
+
+        def ours(yy, carry):
+            part_copy(p * 2 + yy).start()
+            own_out[:, pl.ds(pl.multiple_of((p * 2 + yy) * 256, 256), 256)] = project(p, yy, tp)
+            return carry
+
+        arrived(pairs[2] + pairs[3], p)
+        lax.fori_loop(0, 2, theirs, 0)
+        lax.fori_loop(0, 2, ours, 0)
+
+    def rows_of(core):
+        return pl.ds(pl.multiple_of(core * half, half), half)
+
+    def last_part(yy, low, high):
+        p = m.piece(3)
+        weight = jnp.concatenate([wo[p, yy, 0, low:high, :], wo[p, yy, 1, low:high, :]], axis=1)
+        return lambda core: dot(act[rows_of(core), low:high], weight, ((1,), (0,)))
+
+    def last_begin():
         def body(yy, carry):
-            out_block(m.piece(j), yy)
+            part = last_part(yy, 0, 2 * early)
+            at = pl.ds(pl.multiple_of(yy * 256, 256), 256)
+            acc2[0:half, at] = part(1 - tp)
+            acc2[half:, at] = part(tp)
             return carry
 
-        arrived(pairs[2] + pairs[3], m.piece(j))
+        arrived(pairs[2], m.piece(3))
         lax.fori_loop(0, 2, body, 0)
 
-    def merges(j):
-        def body(yy, carry):
-            merge(m.piece(j), yy)
+    def last_end():
+        b = m.piece(3) * 2
+
+        def theirs(yy, carry):
+            at = pl.ds(pl.multiple_of(yy * 256, 256), 256)
+            part = last_part(yy, 2 * early, 2 * early + 2 * late)
+            psend[b + yy] = (acc2[0:half, at] + part(1 - tp)).astype(jnp.bfloat16)
             return carry
 
-        lax.fori_loop(0, 2, body, 0)
+        def ours(yy, carry):
+            part_copy(b + yy).start()
+            at = pl.ds(pl.multiple_of(yy * 256, 256), 256)
+            part = last_part(yy, 2 * early, 2 * early + 2 * late)
+            own_out[:, pl.ds(pl.multiple_of((b + yy) * 256, 256), 256)] = (acc2[half:, at] + part(tp)).astype(jnp.bfloat16)
+            return carry
+
+        arrived(pairs[3], m.piece(3))
+        lax.fori_loop(0, 2, theirs, 0)
+        lax.fori_loop(0, 2, ours, 0)
+
+    def drain_early():
+        swap.wait_send()
+        stats.wait_send()
+
+        @pl.when(me < 15)
+        def _():
+            halo.wait_send()
+
+        for end in near_ends:
+            end.wait_send()
+        for k in (1, 2, 3):
+            @pl.when(z + k <= 3)
+            def _():
+                far_end(k).wait_send()
+
+        for p in range(4):
+            for f in (b1, b2):
+                f.first_copy(p).wait_send()
+                f.last_copy(p).wait_send()
+            for pair in pairs[:2]:
+                for f in pair:
+                    f.last_copy(p).wait_send()
+        for pair in pairs:
+            for f in pair:
+                f.first_copy(z).wait_send()
+        whole.drain()
+        for pair in lines:
+            for line in pair:
+                line.drain()
+        for j in range(3):
+            for yy in range(2):
+                part_copy(m.piece(j) * 2 + yy).wait()
 
     out_pieces(0)
     out_pieces(1)
-    merges(0)
-    pass_on(3, 2)
+    pass_on(3, 3)
     out_pieces(2)
-    merges(1)
-    pass_on(3, 3)
-    merges(2)
-    out_pieces(3)
-    merges(3)
-
-    swap.wait_send()
-    stats.wait_send()
-
-    @pl.when(me < 15)
-    def _():
-        halo.wait_send()
-
-    end_x.wait_send()
-    end_y.wait_send()
-    for k in (1, 2, 3):
-        @pl.when(z + k <= 3)
-        def _():
-            end_copy(2, 4 + k, 1 + k, me + 4 * k).wait_send()
+    last_begin()
+    drain_early()
+    last_end()
 
     for p in range(4):
-        for f in (b1, b2):
-            f.first_copy(p).wait_send()
-            f.last_copy(p).wait_send()
-        for pair in pairs:
+        for pair in pairs[2:]:
             for f in pair:
                 f.last_copy(p).wait_send()
-    for pair in pairs:
-        for f in pair:
-            f.first_copy(z).wait_send()
-    whole.drain()
-    for pair in lines:
-        for line in pair:
-            line.drain()
-    for b in range(8):
-        part_copy(b).wait_send()
-        out_copy(b).wait()
+    for yy in range(2):
+        part_copy(m.piece(3) * 2 + yy).wait()
 
 
 def fused_layer(
@@ -662,11 +694,12 @@
     dma = pltpu.SemaphoreType.DMA
     vm = pl.BlockSpec(memory_space=pltpu.VMEM)
     hbm = pl.BlockSpec(memory_space=pl.ANY)
-    return pl.pallas_call(
+    share = pltpu.VMEM((half, 2 * width), bf16)
+    own, other = pl.pallas_call(
         layer_kernel,
-        out_shape=jax.ShapeDtypeStruct((half, 2 * width), bf16),
+        out_shape=[share, share],
         in_specs=[hbm, vm, hbm, hbm, vm, vm, hbm, hbm, hbm, hbm, hbm, vm, hbm, vm, vm, hbm, hbm],
-        out_specs=hbm,
+        out_specs=[vm, vm],
         scratch_shapes=[
             pltpu.VMEM((4, 2, 2, depth, 5 * n_key), bf16),
             pltpu.VMEM((4, 2, 2, depth, 2 * n_conv), bf16),
@@ -683,9 +716,6 @@
             pltpu.VMEM((rows, n_key), bf16),
             pltpu.VMEM((rows, 2 * n_conv), bf16),
             pltpu.VMEM((8, half, 256), bf16),
-            pltpu.VMEM((8, half, 256), bf16),
-            pltpu.VMEM((8, half, 256), bf16),
-            pltpu.VMEM((8, half, 256), bf16),
             pltpu.VMEM((pad, n_conv), bf16),
             pltpu.VMEM((pad, n_conv), bf16),
             pltpu.VMEM((rows, 128), f32),
@@ -695,14 +725,15 @@
             pltpu.VMEM((1, n_key), f32),
             pltpu.VMEM((HV + 8, n_key), f32),
             dma((11,)), dma((10, 4)), dma((10, 4)), dma((10, 4)), dma((10, 4)), dma((9, 4)), dma((9, 4)), dma((9, 4)),
-            dma((3,)), dma((3,)), dma((5,)), dma((8,)), dma((8,)), dma((8,)), dma((8,)),
+            dma((3,)), dma((3,)), dma((6,)), dma((8,)), dma((8,)), dma((8,)),
         ],
-        compiler_params=pltpu.CompilerParams(collective_id=0, has_side_effects=True, vmem_limit_bytes=67043328),
+        compiler_params=pltpu.CompilerParams(collective_id=0, has_side_effects=True, vmem_limit_bytes=56 * 2**20),
         name="layer",
     )(
         tokens, norm_gain[None, :], w_conv_a, w_conv_gate, conv_weight, conv_gain[None, :], w_query, w_key, w_value,
         w_outgate, w_decay, decay_bias[None, :], decay_extra, head_gain[None, :], init_state, w_out_conv, w_out_gla,
     )
+    return (own.astype(f32) + other.astype(f32)).astype(bf16)
 
 
 def local_kernel(heads, pieces, q_ref, k_ref, v_ref, pre_ref, extra_ref, bias_ref, attn_ref, since_ref, end_ref, log_ref, state, prefix):

time: 139 us -> 133 us (0.957)
  Pallas kernels: 136 us -> 131 us
  local copies, waits for them, and re-layouts: 3.16 us -> 0 us
  other arithmetic: 0 us -> 2.24 us
    pallas_call x1, Pallas kernels: 136 us -> 131 us  [fused_layer(): pl.pallas_call(layer_kernel, out_shape=[share, share], in_specs=[hbm, vm,...]
    unnamed x1 -> x0, local copies, waits for them, and re-layouts: 3.16 us -> none
    convert_element_type x0 -> x1, other arithmetic: none -> 2.24 us  [fused_layer(): return (own.astype(f32) + other.astype(f32)).astype(bf16)]
where the time goes in v2:
time: 133 us
  Pallas kernels  131 us (98%)
  other arithmetic  2.24 us (2%)
    pallas_call x1, Pallas kernels, fused_layer(): pl.pallas_call(layer_kernel, out_shape=[share, share], in_specs=[hbm, vm,...  131 us

profile of v2, /device:TPU:25, one launch (start us, length us, event | category | flops | bytes accessed | tf_op | source)
XLA Modules:
  0.0 132.9 jit_solution(8777550550120014926)
XLA Ops:
  0.0 130.7 %layer.1 = (bf16[512,2048]{1,0:T(8,128)(2,1)S(1)}, bf16[512,2048]{1,0:T(8,128)(2,1)S(1)}) custom-call(bf16[1024,1024]{1,0:T(8,128)(2,1)} %tokens.1, f32[1,2048]{1,0:T(1,128)} %bitcast.4, bf16[128,512]{1,0:T(8,128)(2,1)} %wa.1, bf16[128,512]{1,0:T(8,128)(2,1)} %wg.1, f32[31,512]{1,0:T(8,128)} %taps.1, f32[1,512]{1,0:T(1,128)} %bitcast.5, ...), custom_call_target="tpu_custom_call" | custom-call | tf_op jit(solution)/shard_map/layer/pallas_call | solution.py:698
  130.7 2.2 %add_convert_fusion = bf16[512,2048]{1,0:T(8,128)(2,1)} fusion(bf16[512,2048]{1,0:T(8,128)(2,1)S(1)} %get-tuple-element.8, bf16[512,2048]{1,0:T(8,128)(2,1)S(1)} %get-tuple-element.7), kind=kLoop, calls=%fused_computation | loop fusion | flops 4194304 | bytes 6291456 | tf_op jit(solution)/shard_map/convert_element_type | solution.py:736

commit v3 on v2

--- a/solution.py
+++ b/solution.py
@@ -59,15 +59,25 @@
         every = slice(None)
         return self.view(p, self.m.y, every) if self.first == "x" else self.view(p, every, self.m.x)
 
-    def first_copy(self, p):
-        own = self.own(p)
+    def first_copy(self, p, source=None):
+        own = self.own(p) if source is None else source
+        slot = self.number * 4 + p if self.number < 2 else self.number + 6
         fs, fr = self.sems["first_send"], self.sems["first_recv"]
-        return self.m.copy(own, own, fs.at[self.number, p], fr.at[self.number, p], self.m.other[self.first])
-
-    def last_copy(self, p):
-        pair = self.pair(p)
+        return self.m.copy(own, own, fs.at[self.number], fr.at[slot], self.m.other[self.first])
+
+    def last_copy(self, p, source=None):
+        pair = self.pair(p) if source is None else source
         ls, lr = self.sems["last_send"], self.sems["last_recv"]
-        return self.m.copy(pair, pair, ls.at[self.number, p], lr.at[self.number, p], self.m.other[self.last])
+        return self.m.copy(pair, pair, ls.at[self.number], lr.at[self.number // 2, p], self.m.other[self.last])
+
+    def drain_first(self):
+        if self.number < 2:
+            self.first_copy(0, self.own(slice(None))).wait_send()
+        else:
+            self.first_copy(self.m.z).wait_send()
+
+    def drain_last(self):
+        self.last_copy(0, self.pair(slice(None))).wait_send()
 
 
 class Line:
@@ -76,13 +86,13 @@
 
     def up(self, p):
         return self.m.copy(
-            self.view(p), self.view(p), self.sems["up_send"].at[self.number, p], self.sems["z_recv"].at[self.number, p],
+            self.view(p), self.view(p), self.sems["z_send"].at[self.number, p], self.sems["z_recv"].at[self.number, p],
             self.m.me + 4,
         )
 
     def down(self, p):
         return self.m.copy(
-            self.view(p), self.view(p), self.sems["down_send"].at[self.number, p],
+            self.view(p), self.view(p), self.sems["z_send"].at[self.number, p + 1],
             self.sems["z_recv"].at[self.number, p], self.m.me - 4,
         )
 
@@ -152,7 +162,7 @@
     tokens, gain, wa, wg, taps, conv_gain, wq, wk, wv, wog, wd, bias, extra_in, head_gain, init, woc, wogl, own_out, other_out,
     w1, w2, w3, wo, both, normed, acc1, acc2, acc3, extra, seq, attn, since, act, psend,
     halo_out, halo_in, stat_own, stat_in, packs, state, prefix, before,
-    local, first_send, first_recv, last_send, last_recv, up_send, down_send, z_recv, misc_send, misc_recv, end_send, end_recv,
+    local, first_send, first_recv, last_send, last_recv, z_send, z_recv, misc_send, misc_recv, end_send, end_recv,
     part_send, part_recv,
 ):
     m = Mover()
@@ -165,7 +175,7 @@
     heads = n_key // HK
     sems = dict(
         first_send=first_send, first_recv=first_recv, last_send=last_send, last_recv=last_recv,
-        up_send=up_send, down_send=down_send, z_recv=z_recv,
+        z_send=z_send, z_recv=z_recv,
     )
 
     def lanes(ref, low, size):
@@ -266,9 +276,25 @@
         for f, line in zip(pairs[k], lines[k]):
             line.relay(step, lambda p: f.last_copy(p).start())
 
-    def arrived(flows, p):
-        for f in flows:
-            f.last_copy(p).wait_recv()
+    def relay_only(k, step):
+        for line in lines[k]:
+            line.relay(step, lambda p: None)
+
+    def finish(k, step):
+        for f in pairs[k]:
+            at_step(z, step, lambda p: f.last_copy(p).start())
+
+    def arrived(k, p):
+        every = (p, slice(None), slice(None))
+        both_flows = (
+            w1.at[(*every, slice(None), pl.ds(0, mid))],
+            w2.at[(*every, slice(None), pl.ds(0, n_conv))],
+            w3.at[(*every, slice(None), pl.ds(0, n_key))],
+            wo.at[(*every, pl.ds(0, early), slice(None))],
+            wo.at[(*every, pl.ds(0, late), slice(None))],
+        )[k]
+        flow = b1 if k == 0 else pairs[k - 1][0]
+        flow.last_copy(p, both_flows).wait_recv()
 
     def norm_tiles(low, high):
         def body(i, carry):
@@ -309,23 +335,23 @@
     enter_one(0, 1)
     head_firsts(1)
     head_line(3)
-    arrived((b1, b2), m.piece(0))
+    arrived(0, m.piece(0))
     slab(acc1, w1, m.piece(0), True)
     head_firsts(2)
     begin(2)
     begin(3)
     pass_on(0, 1)
-    arrived((b1, b2), m.piece(1))
+    arrived(0, m.piece(1))
     slab(acc1, w1, m.piece(1), False)
     head_firsts(3)
     enter(1)
     own_last(0)
     pass_on(0, 2)
-    arrived((b1, b2), m.piece(2))
+    arrived(0, m.piece(2))
     slab(acc1, w1, m.piece(2), False)
     pass_on(1, 1)
     enter(2)
-    arrived((b1, b2), m.piece(3))
+    arrived(0, m.piece(3))
     slab(acc1, w1, m.piece(3), False)
 
     state[...] = jnp.zeros_like(state)
@@ -373,12 +399,11 @@
 
         @pl.when(i == blocks // 2)
         def _():
-            own_last(1)
             pass_on(0, 3)
 
         @pl.when(i == blocks - 3)
         def _():
-            pass_on(1, 2)
+            relay_only(1, 2)
 
         return carry
 
@@ -404,17 +429,19 @@
     ]
     pack(0, jnp.exp(prefix[...]), state[...])
 
-    arrived(pairs[0], m.piece(0))
+    arrived(1, m.piece(0))
     slab(acc2, w2, m.piece(0), True)
     for end in near_ends:
         end.start()
+    own_last(1)
+    finish(1, 2)
     pass_on(2, 1)
     enter(3)
-    arrived(pairs[0], m.piece(1))
+    arrived(1, m.piece(1))
     slab(acc2, w2, m.piece(1), False)
-    arrived(pairs[0], m.piece(2))
+    arrived(1, m.piece(2))
     slab(acc2, w2, m.piece(2), False)
-    arrived(pairs[0], m.piece(3))
+    arrived(1, m.piece(3))
     slab(acc2, w2, m.piece(3), False)
     pass_on(1, 3)
     own_last(2)
@@ -493,6 +520,17 @@
         def _():
             pass_on(2, 2)
 
+        @pl.when(i == chunks - 3)
+        def _():
+            join_near()
+
+        @pl.when(i == chunks - 1)
+        def _():
+            for k in (1, 2, 3):
+                @pl.when(z + k <= 3)
+                def _():
+                    far_end(k).start()
+
         return carry
 
     lax.fori_loop(1, chunks, conv_loop, 0)
@@ -511,21 +549,15 @@
 
     pass_on(3, 1)
     own_last(3)
-    arrived(pairs[1], m.piece(0))
+    arrived(2, m.piece(0))
     slab(acc3, w3, m.piece(0), True)
     stats = m.copy(stat_own, stat_in, misc_send.at[2], misc_recv.at[2], me, 1 - tp)
     stats.start()
-    join_near()
-    arrived(pairs[1], m.piece(1))
+    arrived(2, m.piece(1))
     slab(acc3, w3, m.piece(1), False)
-    for k in (1, 2, 3):
-        @pl.when(z + k <= 3)
-        def _():
-            far_end(k).start()
-
-    arrived(pairs[1], m.piece(2))
+    arrived(2, m.piece(2))
     slab(acc3, w3, m.piece(2), False)
-    arrived(pairs[1], m.piece(3))
+    arrived(2, m.piece(3))
     slab(acc3, w3, m.piece(3), False)
     pass_on(2, 3)
     stats.wait_recv()
@@ -568,7 +600,7 @@
 
     def part_copy(b):
         at = pl.ds(pl.multiple_of(b * 256, 256), 256)
-        return m.copy(psend.at[b], other_out.at[:, at], part_send.at[b], part_recv.at[b], me, 1 - tp)
+        return m.copy(psend.at[b], other_out.at[:, at], part_send, part_recv, me, 1 - tp)
 
     def project(p, yy, core):
         weight = jnp.concatenate([wo[p, yy, 0], wo[p, yy, 1]], axis=1)
@@ -587,7 +619,8 @@
             own_out[:, pl.ds(pl.multiple_of((p * 2 + yy) * 256, 256), 256)] = project(p, yy, tp)
             return carry
 
-        arrived(pairs[2] + pairs[3], p)
+        arrived(3, p)
+        arrived(4, p)
         lax.fori_loop(0, 2, theirs, 0)
         lax.fori_loop(0, 2, ours, 0)
 
@@ -607,7 +640,7 @@
             acc2[half:, at] = part(tp)
             return carry
 
-        arrived(pairs[2], m.piece(3))
+        arrived(3, m.piece(3))
         lax.fori_loop(0, 2, body, 0)
 
     def last_end():
@@ -626,7 +659,7 @@
             own_out[:, pl.ds(pl.multiple_of((b + yy) * 256, 256), 256)] = (acc2[half:, at] + part(tp)).astype(jnp.bfloat16)
             return carry
 
-        arrived(pairs[3], m.piece(3))
+        arrived(4, m.piece(3))
         lax.fori_loop(0, 2, theirs, 0)
         lax.fori_loop(0, 2, ours, 0)
 
@@ -645,38 +678,28 @@
             def _():
                 far_end(k).wait_send()
 
-        for p in range(4):
-            for f in (b1, b2):
-                f.first_copy(p).wait_send()
-                f.last_copy(p).wait_send()
-            for pair in pairs[:2]:
-                for f in pair:
-                    f.last_copy(p).wait_send()
-        for pair in pairs:
-            for f in pair:
-                f.first_copy(z).wait_send()
+        for f in (b1, b2, *pairs[0], *pairs[1]):
+            f.drain_first()
+            f.drain_last()
+        for f in (*pairs[2], *pairs[3]):
+            f.drain_first()
         whole.drain()
         for pair in lines:
             for line in pair:
                 line.drain()
-        for j in range(3):
-            for yy in range(2):
-                part_copy(m.piece(j) * 2 + yy).wait()
 
     out_pieces(0)
+    pass_on(3, 3)
     out_pieces(1)
-    pass_on(3, 3)
     out_pieces(2)
     last_begin()
     drain_early()
     last_end()
 
-    for p in range(4):
-        for pair in pairs[2:]:
-            for f in pair:
-                f.last_copy(p).wait_send()
-    for yy in range(2):
-        part_copy(m.piece(3) * 2 + yy).wait()
+    for f in (*pairs[2], *pairs[3]):
+        f.drain_last()
+    m.copy(psend, psend, part_send, part_recv, me, 1 - tp).wait_send()
+    m.copy(other_out, other_out, part_send, part_recv, me, 1 - tp).wait_recv()
 
 
 def fused_layer(
@@ -724,8 +747,8 @@
             pltpu.VMEM((HV, n_key), f32),
             pltpu.VMEM((1, n_key), f32),
             pltpu.VMEM((HV + 8, n_key), f32),
-            dma((11,)), dma((10, 4)), dma((10, 4)), dma((10, 4)), dma((10, 4)), dma((9, 4)), dma((9, 4)), dma((9, 4)),
-            dma((3,)), dma((3,)), dma((6,)), dma((8,)), dma((8,)), dma((8,)),
+            dma((11,)), dma((10,)), dma((16,)), dma((10,)), dma((5, 4)), dma((9, 5)), dma((9, 4)),
+            dma((3,)), dma((3,)), dma((6,)), dma((8,)), dma(()), dma(()),
         ],
         compiler_params=pltpu.CompilerParams(collective_id=0, has_side_effects=True, vmem_limit_bytes=56 * 2**20),
         name="layer",

time: 133 us -> 131 us (0.985); the launches traced: 133 us -> 129 us
  Pallas kernels: 131 us -> 126 us
    pallas_call x1, Pallas kernels: 131 us -> 126 us  [fused_layer(): pl.pallas_call(layer_kernel, out_shape=[share, share], in_specs=[hbm, vm,...]
where the time goes in v3:
time: 131 us; the launch traced here: 129 us
  Pallas kernels  126 us (96%)
  other arithmetic  2.24 us (2%)
    pallas_call x1, Pallas kernels, fused_layer(): pl.pallas_call(layer_kernel, out_shape=[share, share], in_specs=[hbm, vm,...  126 us

profile of v3, /device:TPU:25, one launch (start us, length us, event | category | flops | bytes accessed | tf_op | source)
XLA Modules:
  0.0 128.5 jit_solution(9081423011443530690)
XLA Ops:
  0.0 126.3 %layer.1 = (bf16[512,2048]{1,0:T(8,128)(2,1)S(1)}, bf16[512,2048]{1,0:T(8,128)(2,1)S(1)}) custom-call(bf16[1024,1024]{1,0:T(8,128)(2,1)} %tokens.1, f32[1,2048]{1,0:T(1,128)} %bitcast.4, bf16[128,512]{1,0:T(8,128)(2,1)} %wa.1, bf16[128,512]{1,0:T(8,128)(2,1)} %wg.1, f32[31,512]{1,0:T(8,128)} %taps.1, f32[1,512]{1,0:T(1,128)} %bitcast.5, ...), custom_call_target="tpu_custom_call" | custom-call | tf_op jit(solution)/shard_map/layer/pallas_call | solution.py:721
  126.3 2.2 %add_convert_fusion = bf16[512,2048]{1,0:T(8,128)(2,1)} fusion(bf16[512,2048]{1,0:T(8,128)(2,1)S(1)} %get-tuple-element.8, bf16[512,2048]{1,0:T(8,128)(2,1)S(1)} %get-tuple-element.7), kind=kLoop, calls=%fused_computation | loop fusion | flops 4194304 | bytes 6291456 | tf_op jit(solution)/shard_map/convert_element_type | solution.py:759

commit v4 on v3

--- a/solution.py
+++ b/solution.py
@@ -216,11 +216,29 @@
         load.start()
 
     barrier = pltpu.get_barrier_semaphore()
-    partners = [(m.other["x"], tp), (m.other["y"], tp), (m.across, tp), (me, 1 - tp)]
-    partners += [((me + k) % 16, tp) for k in (4, 8, 12, 1, 15)]
-    for place, core in partners:
+    def greet(place, core):
         pl.semaphore_signal(barrier, inc=1, device_id=(place, core), device_id_type=MESH)
-    pl.semaphore_wait(barrier, len(partners))
+
+    for place, core in ((m.other["x"], tp), (m.other["y"], tp), (me, 1 - tp)):
+        greet(place, core)
+
+    @pl.when(z < 3)
+    def _():
+        greet(me + 4, tp)
+
+    @pl.when(z > 0)
+    def _():
+        greet(me - 4, tp)
+
+    at_end = (z == 0) | (z == 3)
+
+    @pl.when(at_end)
+    def _():
+        pl.semaphore_wait(barrier, 4)
+
+    @pl.when(jnp.logical_not(at_end))
+    def _():
+        pl.semaphore_wait(barrier, 5)
 
     for i in range(4):
         loads[i].wait()

time: 131 us -> 128 us (0.977); the launches traced: 129 us -> 128 us
  no operation moved by 1% of the time
where the time goes in v4:
time: 128 us
  Pallas kernels  125 us (98%)
  other arithmetic  2.24 us (2%)
    pallas_call x1, Pallas kernels, fused_layer(): pl.pallas_call(layer_kernel, out_shape=[share, share], in_specs=[hbm, vm,...  125 us

profile of v4, /device:TPU:25, one launch (start us, length us, event | category | flops | bytes accessed | tf_op | source)
XLA Modules:
  0.0 127.5 jit_solution(12278488787378177581)
XLA Ops:
  0.0 125.3 %layer.1 = (bf16[512,2048]{1,0:T(8,128)(2,1)S(1)}, bf16[512,2048]{1,0:T(8,128)(2,1)S(1)}) custom-call(bf16[1024,1024]{1,0:T(8,128)(2,1)} %tokens.1, f32[1,2048]{1,0:T(1,128)} %bitcast.4, bf16[128,512]{1,0:T(8,128)(2,1)} %wa.1, bf16[128,512]{1,0:T(8,128)(2,1)} %wg.1, f32[31,512]{1,0:T(8,128)} %taps.1, f32[1,512]{1,0:T(1,128)} %bitcast.5, ...), custom_call_target="tpu_custom_call" | custom-call | tf_op jit(solution)/shard_map/layer/pallas_call | solution.py:739
  125.3 2.2 %add_convert_fusion = bf16[512,2048]{1,0:T(8,128)(2,1)} fusion(bf16[512,2048]{1,0:T(8,128)(2,1)S(1)} %get-tuple-element.8, bf16[512,2048]{1,0:T(8,128)(2,1)S(1)} %get-tuple-element.7), kind=kLoop, calls=%fused_computation | loop fusion | flops 4194304 | bytes 6291456 | tf_op jit(solution)/shard_map/convert_element_type | solution.py:777

commit v5 on v4

--- a/solution.py
+++ b/solution.py
@@ -534,7 +534,7 @@
     def conv_loop(i, carry):
         conv_chunk(i)
 
-        @pl.when(i == chunks // 2)
+        @pl.when((i == chunks // 2) & jnp.logical_not(at_end))
         def _():
             pass_on(2, 2)
 
@@ -553,32 +553,33 @@
 
     lax.fori_loop(1, chunks, conv_loop, 0)
 
-    @pl.when(me > 0)
-    def _():
-        halo.wait_recv()
-        for c in range(n_conv // 128):
-            seq[c, 0:pad, :] = halo_in[:, c * 128 : (c + 1) * 128].astype(jnp.float32)
-
-    @pl.when(me == 0)
-    def _():
-        seq[:, 0:pad, :] = jnp.zeros((n_conv // 128, pad, 128), jnp.float32)
-
-    lax.fori_loop(0, 1, conv_loop, 0)
-
+    @pl.when(at_end)
+    def _():
+        pass_on(2, 2)
+
+    arrived(2, m.piece(0))
+    slab(acc3, w3, m.piece(0), True)
     pass_on(3, 1)
     own_last(3)
-    arrived(2, m.piece(0))
-    slab(acc3, w3, m.piece(0), True)
-    stats = m.copy(stat_own, stat_in, misc_send.at[2], misc_recv.at[2], me, 1 - tp)
-    stats.start()
     arrived(2, m.piece(1))
     slab(acc3, w3, m.piece(1), False)
     arrived(2, m.piece(2))
     slab(acc3, w3, m.piece(2), False)
     arrived(2, m.piece(3))
     slab(acc3, w3, m.piece(3), False)
-    pass_on(2, 3)
-    stats.wait_recv()
+    @pl.when(me > 0)
+    def _():
+        halo.wait_recv()
+        for c in range(n_conv // 128):
+            seq[c, 0:pad, :] = halo_in[:, c * 128 : (c + 1) * 128].astype(jnp.float32)
+
+    @pl.when(me == 0)
+    def _():
+        seq[:, 0:pad, :] = jnp.zeros((n_conv // 128, pad, 128), jnp.float32)
+
+    lax.fori_loop(0, 1, conv_loop, 0)
+
+    stats = m.copy(stat_own, stat_in, misc_send.at[2], misc_recv.at[2], me, 1 - tp)
 
     def conv_finish(i, carry):
         at = pl.ds(pl.multiple_of(i * 128, 128), 128)
@@ -590,8 +591,16 @@
         act[at, 0:n_conv] = (value * jax.nn.sigmoid(value)).astype(jnp.bfloat16)
         return carry
 
+    stats.start()
+
+    @pl.when(jnp.logical_not(at_end))
+    def _():
+        pass_on(3, 2)
+
+    stats.wait_recv()
     lax.fori_loop(0, chunks, conv_finish, 0)
-    pass_on(3, 2)
+    pass_on(2, 3)
+
     for k in (1, 2, 3):
         @pl.when(z - k >= 0)
         def _():
@@ -707,10 +716,15 @@
                 line.drain()
 
     out_pieces(0)
+
+    @pl.when(at_end)
+    def _():
+        pass_on(3, 2)
+
+    out_pieces(1)
     pass_on(3, 3)
-    out_pieces(1)
+    last_begin()
     out_pieces(2)
-    last_begin()
     drain_early()
     last_end()
 

time: 128 us -> 126 us (0.984)
    pallas_call x1, Pallas kernels: 125 us -> 124 us  [fused_layer(): pl.pallas_call(layer_kernel, out_shape=[share, share], in_specs=[hbm, vm,...]
where the time goes in v5:
time: 126 us
  Pallas kernels  124 us (98%)
  other arithmetic  2.24 us (2%)
    pallas_call x1, Pallas kernels, fused_layer(): pl.pallas_call(layer_kernel, out_shape=[share, share], in_specs=[hbm, vm,...  124 us

profile of v5, /device:TPU:25, one launch (start us, length us, event | category | flops | bytes accessed | tf_op | source)
XLA Modules:
  0.0 126.0 jit_solution(4068062227298988883)
XLA Ops:
  0.0 123.7 %layer.1 = (bf16[512,2048]{1,0:T(8,128)(2,1)S(1)}, bf16[512,2048]{1,0:T(8,128)(2,1)S(1)}) custom-call(bf16[1024,1024]{1,0:T(8,128)(2,1)} %tokens.1, f32[1,2048]{1,0:T(1,128)} %bitcast.4, bf16[128,512]{1,0:T(8,128)(2,1)} %wa.1, bf16[128,512]{1,0:T(8,128)(2,1)} %wg.1, f32[31,512]{1,0:T(8,128)} %taps.1, f32[1,512]{1,0:T(1,128)} %bitcast.5, ...), custom_call_target="tpu_custom_call" | custom-call | tf_op jit(solution)/shard_map/layer/pallas_call | solution.py:753
  123.7 2.2 %add_convert_fusion = bf16[512,2048]{1,0:T(8,128)(2,1)} fusion(bf16[512,2048]{1,0:T(8,128)(2,1)S(1)} %get-tuple-element.8, bf16[512,2048]{1,0:T(8,128)(2,1)S(1)} %get-tuple-element.7), kind=kLoop, calls=%fused_computation | loop fusion | flops 4194304 | bytes 6291456 | tf_op jit(solution)/shard_map/convert_element_type | solution.py:791

commit v6 on v5

--- a/solution.py
+++ b/solution.py
@@ -185,7 +185,7 @@
         return lambda p, yy, xx: wo.at[p, yy, xx, pl.ds(low, size), :]
 
     mid = w1.shape[-1] // 2
-    late = wo.shape[3] // 8
+    late = wo.shape[3] // 4
     early = wo.shape[3] // 2 - late
     b1 = Flow(m, 0, lanes(w1, 0, mid), "x", sems)
     b2 = Flow(m, 1, lanes(w1, mid, mid), "y", sems)

time: 126 us -> 126 us (level); the launches traced: 126 us -> 125 us
  Pallas kernels: 124 us -> 122 us
    pallas_call x1, Pallas kernels: 124 us -> 122 us  [fused_layer(): pl.pallas_call(layer_kernel, out_shape=[share, share], in_specs=[hbm, vm,...]
where the time goes in v6:
time: 126 us; the launch traced here: 125 us
  Pallas kernels  122 us (97%)
  other arithmetic  2.24 us (2%)
    pallas_call x1, Pallas kernels, fused_layer(): pl.pallas_call(layer_kernel, out_shape=[share, share], in_specs=[hbm, vm,...  122 us

profile of v6, /device:TPU:25, one launch (start us, length us, event | category | flops | bytes accessed | tf_op | source)
XLA Modules:
  0.0 124.7 jit_solution(7165515005696537198)
XLA Ops:
  0.0 122.4 %layer.1 = (bf16[512,2048]{1,0:T(8,128)(2,1)S(1)}, bf16[512,2048]{1,0:T(8,128)(2,1)S(1)}) custom-call(bf16[1024,1024]{1,0:T(8,128)(2,1)} %tokens.1, f32[1,2048]{1,0:T(1,128)} %bitcast.4, bf16[128,512]{1,0:T(8,128)(2,1)} %wa.1, bf16[128,512]{1,0:T(8,128)(2,1)} %wg.1, f32[31,512]{1,0:T(8,128)} %taps.1, f32[1,512]{1,0:T(1,128)} %bitcast.5, ...), custom_call_target="tpu_custom_call" | custom-call | tf_op jit(solution)/shard_map/layer/pallas_call | solution.py:753
  122.4 2.2 %add_convert_fusion = bf16[512,2048]{1,0:T(8,128)(2,1)} fusion(bf16[512,2048]{1,0:T(8,128)(2,1)S(1)} %get-tuple-element.8, bf16[512,2048]{1,0:T(8,128)(2,1)S(1)} %get-tuple-element.7), kind=kLoop, calls=%fused_computation | loop fusion | flops 4194304 | bytes 6291456 | tf_op jit(solution)/shard_map/convert_element_type | solution.py:791

commit v7 on v6

--- a/solution.py
+++ b/solution.py
@@ -419,6 +419,10 @@
         def _():
             pass_on(0, 3)
 
+        @pl.when((i == blocks // 2) & at_end)
+        def _():
+            own_last(1)
+
         @pl.when(i == blocks - 3)
         def _():
             relay_only(1, 2)
@@ -451,7 +455,11 @@
     slab(acc2, w2, m.piece(0), True)
     for end in near_ends:
         end.start()
-    own_last(1)
+
+    @pl.when(jnp.logical_not(at_end))
+    def _():
+        own_last(1)
+
     finish(1, 2)
     pass_on(2, 1)
     enter(3)

time: 126 us -> 126 us (level)
  no operation moved by 1% of the time
where the time goes in v7:
time: 126 us; the launch traced here: 125 us
  Pallas kernels  122 us (97%)
  other arithmetic  2.24 us (2%)
    pallas_call x1, Pallas kernels, fused_layer(): pl.pallas_call(layer_kernel, out_shape=[share, share], in_specs=[hbm, vm,...  122 us

profile of v7, /device:TPU:25, one launch (start us, length us, event | category | flops | bytes accessed | tf_op | source)
XLA Modules:
  0.0 124.7 jit_solution(14546539490585776855)
XLA Ops:
  0.0 122.4 %layer.1 = (bf16[512,2048]{1,0:T(8,128)(2,1)S(1)}, bf16[512,2048]{1,0:T(8,128)(2,1)S(1)}) custom-call(bf16[1024,1024]{1,0:T(8,128)(2,1)} %tokens.1, f32[1,2048]{1,0:T(1,128)} %bitcast.4, bf16[128,512]{1,0:T(8,128)(2,1)} %wa.1, bf16[128,512]{1,0:T(8,128)(2,1)} %wg.1, f32[31,512]{1,0:T(8,128)} %taps.1, f32[1,512]{1,0:T(1,128)} %bitcast.5, ...), custom_call_target="tpu_custom_call" | custom-call | tf_op jit(solution)/shard_map/layer/pallas_call | solution.py:761
  122.4 2.2 %add_convert_fusion = bf16[512,2048]{1,0:T(8,128)(2,1)} fusion(bf16[512,2048]{1,0:T(8,128)(2,1)S(1)} %get-tuple-element.8, bf16[512,2048]{1,0:T(8,128)(2,1)S(1)} %get-tuple-element.7), kind=kLoop, calls=%fused_computation | loop fusion | flops 4194304 | bytes 6291456 | tf_op jit(solution)/shard_map/convert_element_type | solution.py:799
